TPU v7x, 512 devices: a whole 4x8x8 slice. The times are simulated.
512 devices in a mesh: sp: 32 (over z, x), tp: 16 (over y, core).
Axes of the slice: x: 4, y: 8, z: 8, core: 2. Of those that a mesh axis runs over, the one named last changes fastest.
Arguments:
- mid_state: bfloat16 [8192, 2048], P('sp'), may hold values from -6 to 6
- conv_pre: bfloat16 [8192, 1024], P('sp', 'tp'), may hold values from -8 to 8
- conv_taps: bfloat16 [31, 1024], P(None, 'tp'), may hold values from -1 to 1
- out_proj: bfloat16 [1024, 2048], P('tp'), may hold values from -0.1875 to 0.1875
- route_expert: int32 [8192, 2], P('sp'), may hold values from 0 to 31, as said below
- route_weight: float32 [8192, 2], P('sp'), may hold values from 0.1 to 1
- gate_w: bfloat16 [32, 2048, 2048], P('sp', None, 'tp'), may hold values from -0.125 to 0.125
- up_w: bfloat16 [32, 2048, 2048], P('sp', None, 'tp'), may hold values from -0.125 to 0.125
- down_w: bfloat16 [32, 2048, 2048], P('sp', 'tp'), may hold values from -0.125 to 0.125
- cotangent: bfloat16 [8192, 2048], P('sp'), may hold values from -6 to 6
Outputs:
- grad_gate: bfloat16 [32, 2048, 2048], P('sp', None, 'tp')
- grad_up: bfloat16 [32, 2048, 2048], P('sp', None, 'tp')
- grad_down: bfloat16 [32, 2048, 2048], P('sp', 'tp')
- grad_proj: float32 [2048, 1024], P('sp', 'tp')
- conv_input_grad: float32 [8192, 1024], P('sp', 'tp')
Inputs may be any that keep to these rules, and one draw needn't show every extreme that they name: `route_expert`: the two experts of a token are different and lie in one group of 32 // 4 consecutive experts; in every draw some expert is named by more than 17 routes of every aligned block of 256 tokens.
All inputs are finite; a program needn't handle non-finite values.
Results may differ from a plain program's by a relative error of at most 0.02.
Values may be sent and summed in bfloat16 or wider, within the bound.
A program may use at most 128 MiB of HBM per device.

v0:
```python
import jax
import jax.numpy as jnp
from jax import lax
from jax.sharding import PartitionSpec as P

D = 2048
KERNEL = 31
TOP = 2


def in_one_piece(arrays, axis, split_dim, concat_dim, along):
    widths = [a.shape[along] for a in arrays]
    both = jnp.concatenate(arrays, axis=along)
    whole = lax.all_to_all(both, axis, split_axis=split_dim, concat_axis=concat_dim, tiled=True)
    return tuple(jnp.split(whole, [sum(widths[:k]) for k in range(1, len(widths))], axis=along))


def sent_together(arrays, axis, dim, along):
    widths = [a.shape[along] for a in arrays]
    both = jnp.concatenate(arrays, axis=along)
    whole = lax.all_gather(both, axis, axis=dim, tiled=True)
    return tuple(jnp.split(whole, [sum(widths[:k]) for k in range(1, len(widths))], axis=along))


def split_up(shard, dim, peers):
    shape = shard.shape
    parts = shard.reshape(*shape[:dim], peers, shape[dim] // peers, *shape[dim + 1 :])
    return jnp.moveaxis(parts, dim, 0)


def sum_at_owner(shard, axis, dim):
    peers = lax.axis_size(axis)
    parts = lax.all_to_all(split_up(shard, dim, peers), axis, 0, 0, tiled=True)
    return jnp.sum(parts.astype(jnp.float32), axis=0)


def passed_along(value, axis, steps):
    count = lax.axis_size(axis)
    initial, last = (max(0, -steps), min(count, count - steps))
    return lax.ppermute(value, axis, [(source, source + steps) for source in range(initial, last)])


def silu_slope(value):
    sig = jax.nn.sigmoid(value)
    return sig * (1.0 + value * (1.0 - sig))


def body(
    mid_state,
    conv_pre,
    conv_taps,
    out_proj,
    route_expert,
    route_weight,
    gate_w,
    up_w,
    down_w,
    cotangent,
):
    groups = lax.axis_size("sp")
    token_count = mid_state.shape[0]
    slot_count = 17 * token_count * TOP // (16 * groups)
    flat_routes = route_expert.reshape(-1)
    one_hot_table = (flat_routes[:, None] == jnp.arange(groups, dtype=jnp.int32)[None, :]).astype(
        jnp.int32
    )
    slot_rank = jnp.sum(jnp.cumsum(one_hot_table, axis=0) * one_hot_table, axis=1) - 1
    kept_mask = slot_rank < slot_count
    slot_index = jnp.where(kept_mask, flat_routes * slot_count + slot_rank, groups * slot_count)
    token_ids = jnp.arange(token_count * TOP, dtype=jnp.int32) // TOP
    route_cot = (
        route_weight.reshape(-1)[:, None] * cotangent[token_ids].astype(jnp.float32)
    ).astype(jnp.bfloat16)
    send_inputs = (
        jnp.zeros((groups * slot_count, D), jnp.bfloat16)
        .at[slot_index]
        .set(mid_state[token_ids], mode="drop")
        .reshape(groups, slot_count, D)
    )
    send_seeds = (
        jnp.zeros((groups * slot_count, D), jnp.bfloat16)
        .at[slot_index]
        .set(route_cot, mode="drop")
        .reshape(groups, slot_count, D)
    )
    column_width = D // lax.axis_size("tp")
    column_start = lax.axis_index("tp") * column_width
    part_inputs = lax.dynamic_slice_in_dim(send_inputs, column_start, column_width, 2)
    part_seeds = lax.dynamic_slice_in_dim(send_seeds, column_start, column_width, 2)
    got_parts = in_one_piece((part_inputs, part_seeds), "sp", 0, 0, 1)
    got_inputs, got_seeds = sent_together((got_parts[0], got_parts[1]), "tp", 2, 0)
    inputs = got_inputs.reshape(groups * slot_count, D)
    seeds = got_seeds.reshape(groups * slot_count, D)
    gate_mat = gate_w[0]
    up_mat = up_w[0]
    down_mat = down_w[0]
    gate_pre = jnp.dot(inputs, gate_mat, preferred_element_type=jnp.float32)
    up_pre = jnp.dot(inputs, up_mat, preferred_element_type=jnp.float32)
    gate_act = jax.nn.silu(gate_pre)
    hidden = (gate_act * up_pre).astype(jnp.bfloat16)
    hidden_grad = lax.dot_general(
        seeds, down_mat, (((1,), (1,)), ((), ())), preferred_element_type=jnp.float32
    )
    gate_grad = (hidden_grad * up_pre * silu_slope(gate_pre)).astype(jnp.bfloat16)
    up_grad = (hidden_grad * gate_act).astype(jnp.bfloat16)
    grad_down = lax.dot_general(
        hidden, seeds, (((0,), (0,)), ((), ())), preferred_element_type=jnp.float32
    ).astype(jnp.bfloat16)
    grad_gate = lax.dot_general(
        inputs, gate_grad, (((0,), (0,)), ((), ())), preferred_element_type=jnp.float32
    ).astype(jnp.bfloat16)
    grad_up = lax.dot_general(
        inputs, up_grad, (((0,), (0,)), ((), ())), preferred_element_type=jnp.float32
    ).astype(jnp.bfloat16)
    weight_results = (grad_gate, grad_up, grad_down)
    partial_value = lax.dot_general(
        gate_grad, gate_mat, (((1,), (1,)), ((), ())), preferred_element_type=jnp.float32
    )
    partial_value = partial_value + lax.dot_general(
        up_grad, up_mat, (((1,), (1,)), ((), ())), preferred_element_type=jnp.float32
    )
    partial_value = partial_value.astype(jnp.bfloat16).astype(jnp.float32)
    safe_index = jnp.minimum(slot_index, groups * slot_count - 1)
    slice_width = D // lax.axis_size("tp")
    summed = sum_at_owner(partial_value.astype(jnp.bfloat16), "tp", 1).astype(jnp.bfloat16)
    returned = lax.all_to_all(
        summed.reshape(groups, slot_count, slice_width),
        "sp",
        split_axis=0,
        concat_axis=0,
        tiled=True,
    ).reshape(groups * slot_count, slice_width)
    picked = jnp.where(
        kept_mask[:, None], returned[safe_index].astype(jnp.float32), jnp.float32(0.0)
    )
    moe_grad = jnp.sum(picked.reshape(token_count, TOP, slice_width), axis=1)
    own_cot = lax.dynamic_slice_in_dim(
        cotangent, lax.axis_index("tp") * slice_width, slice_width, 1
    )
    mid_part = (own_cot.astype(jnp.float32) + moe_grad).astype(jnp.bfloat16)
    mid_grad = lax.all_gather(mid_part, "tp", axis=1, tiled=True)
    grad_gate, grad_up, grad_down = weight_results
    pre_float = conv_pre.astype(jnp.float32)
    activated = jax.nn.silu(pre_float).astype(jnp.bfloat16)
    mixed_grad = lax.dot_general(
        mid_grad, out_proj, (((1,), (1,)), ((), ())), preferred_element_type=jnp.float32
    )
    conv_grad = (mixed_grad * silu_slope(pre_float)).astype(jnp.bfloat16)
    next_head = passed_along(conv_grad[: KERNEL - 1], "sp", -1)
    extended = jnp.concatenate([conv_grad, next_head], axis=0).astype(jnp.float32)
    conv_input_grad = jnp.zeros(conv_grad.shape, jnp.float32)
    for lag_index in range(KERNEL):
        conv_input_grad = (
            conv_input_grad
            + conv_taps[lag_index].astype(jnp.float32)[None, :]
            * extended[lag_index : lag_index + token_count]
        )
    grad_proj = sum_at_owner(
        lax.dot_general(
            mid_grad, activated, (((0,), (0,)), ((), ())), preferred_element_type=jnp.float32
        ).astype(jnp.bfloat16),
        "sp",
        0,
    )
    return (grad_gate[None], grad_up[None], grad_down[None], grad_proj, conv_input_grad)


def solution(mesh):
    placed = (
        P("sp", None),
        P("sp", "tp"),
        P(None, "tp"),
        P("tp", None),
        P("sp", None),
        P("sp", None),
        P("sp", None, "tp"),
        P("sp", None, "tp"),
        P("sp", "tp", None),
        P("sp", None),
    )
    return jax.shard_map(
        body,
        mesh=mesh,
        in_specs=placed,
        out_specs=(
            P("sp", None, "tp"),
            P("sp", None, "tp"),
            P("sp", "tp", None),
            P("sp", "tp"),
            P("sp", "tp"),
        ),
        check_vma=False,
    )
```

profile of v0, /device:TPU:8, one launch (start us, length us, event | category | flops | bytes accessed | tf_op | source)
XLA Modules:
  0.0 308.6 jit_solution(7336341047783768166)
XLA Ops:
  13.1 10.4 %scatter_custom_fusion.1 = bf16[544,2048]{1,0:T(8,128)(2,1)S(1)} fusion(s32[512]{0:T(512)S(1)} %bitcast.169, f32[512]{0:T(512)S(1)} %mul.476, bf16[]{:T(256)} %constant.19.clone.1, bf16[256,2048]{1,0:T(8,128)(2,1)} %param.19, s32[1024]{0:T(1024)S(1)} %pad_clamp_fusion.1), kind=kCustom, calls=%fused_computation.15 | custom fusion | flops 3145728 | bytes 3282946 | tf_op jit(solution)/shard_map/scatter | solution.py:83
  23.5 2.5 reshape.173
  26.0 10.9 %scatter_custom_fusion = bf16[544,2048]{1,0:T(8,128)(2,1)S(1)} fusion(s32[512]{0:T(512)S(1)} %bitcast.170, bf16[256,2048]{1,0:T(8,128)(2,1)S(1)} %copy-done, s32[1024]{0:T(1024)S(1)} %pad_clamp_fusion.1, bf16[]{:T(256)} %constant.19.clone.1), kind=kCustom, calls=%fused_computation.16 | custom fusion | bytes 2228226 | tf_op jit(solution)/shard_map/scatter | solution.py:77
  36.9 2.5 reshape.172
  40.6 27.0 %all_to_all.20 = bf16[32,34,128]{2,1,0:T(8,128)(2,1)S(1)} all-to-all(bf16[32,34,128]{2,1,0:T(8,128)(2,1)S(1)} %pad_maximum_fusion.1), channel_id=1, replica_groups=mesh['sp'=32,'tp'=16] {'sp'}, dimensions={0} | all-to-all | bytes 557056 | tf_op jit(solution)/shard_map/all_to_all | solution.py:14
  68.5 55.8 %all-gather.3.cloned.1.call-done = bf16[64,17,2048]{2,1,0:T(8,128)(2,1)} async-done(((bf16[64,17,128]{2,1,0:T(8,128)(2,1)}), bf16[64,17,2048]{2,1,0:T(8,128)(2,1)}) %all-gather.3.cloned.1.call-update) | async-done | bytes 4456464 | tf_op jit(solution)/shard_map/all_gather | solution.py:21
  124.3 6.6 %fusion.67 = (bf16[32,17,2048]{2,1,0:T(8,128)(2,1)}, bf16[32,17,2048]{2,1,0:T(8,128)(2,1)}) fusion(bf16[64,17,2048]{2,1,0:T(8,128)(2,1)} %all-gather.3.cloned.1.call-done), kind=kLoop, calls=%fused_computation.173 | loop fusion | bytes 8912896 | tf_op jit(solution)/shard_map/split | solution.py:22
  131.0 3.0 reshape.174
  134.0 1.8 fusion.13
  135.8 1.5 fusion.16
  137.3 4.4 %reshape.175 = bf16[544,2048]{1,0:T(8,128)(2,1)} reshape(bf16[32,17,2048]{2,1,0:T(8,128)(2,1)} %get-tuple-element.12) | data formatting | bytes 4456448 | tf_op jit(solution)/shard_map/reshape | solution.py:93
  141.7 2.6 multiply_convert_fusion.3
  146.6 57.0 %all_to_all.21 = bf16[16,544,128]{2,1,0:T(8,128)(2,1)} all-to-all(bf16[16,544,128]{2,1,0:T(8,128)(2,1)S(1)} %bitcast.163), channel_id=1, replica_groups=mesh['sp'=32,'tp'=16] {'tp'}, dimensions={0} | all-to-all | bytes 4456448 | tf_op jit(solution)/shard_map/all_to_all | solution.py:33
  203.6 2.0 reduce_sum.40
  206.3 10.3 %all-to-all-start.2 = ((bf16[32,17,128]{2,1,0:T(8,128)(2,1)}), bf16[32,17,128]{2,1,0:T(8,128)(2,1)}, u32[]{:S(2)}, u32[]{:S(2)}) async-start(bf16[32,17,128]{2,1,0:T(8,128)(2,1)} %reshape.177), calls=%async_computation.2 | async-start | bytes 393216 | tf_op jit(solution)/shard_map/all_to_all | solution.py:126
  218.1 11.0 %all-to-all-done.2 = bf16[32,17,128]{2,1,0:T(8,128)(2,1)} async-done(((bf16[32,17,128]{2,1,0:T(8,128)(2,1)}), bf16[32,17,128]{2,1,0:T(8,128)(2,1)}, u32[]{:S(2)}, u32[]{:S(2)}) %all-to-all-start.2) | async-done | bytes 139296 | tf_op jit(solution)/shard_map/all_to_all | solution.py:126
  230.0 1.5 gather_fusion
  231.5 1.2 fusion.21
  232.8 1.5 add_convert_fusion.1
  235.6 2.8 fusion.1
  238.4 1.4 fusion.2
  239.8 25.7 %all-gather.5.cloned.1.call-done = bf16[256,2048]{1,0:T(8,128)(2,1)} async-done(((bf16[256,128]{1,0:T(8,128)(2,1)}), bf16[256,2048]{1,0:T(8,128)(2,1)}) %all-gather.5.cloned.1.call-update) | async-done | bytes 1048592 | tf_op jit(solution)/shard_map/all_gather | solution.py:141
  265.6 1.7 fusion.8
  267.9 1.3 collective-permute-start
  269.2 1.5 convolution_convert_fusion.3
  270.8 1.3 reshape.179
  272.1 2.0 copy.36
  274.1 2.1 reshape.269
  276.2 11.6 %all-to-all-start.3 = ((bf16[32,2,2048]{2,1,0:T(2,128)(2,1)}), bf16[32,2,2048]{2,1,0:T(2,128)(2,1)S(1)}, u32[]{:S(2)}, u32[]{:S(2)}) async-start(bf16[32,2,2048]{2,1,0:T(2,128)(2,1)} %reshape.269), calls=%async_computation.3 | async-start | bytes 524288 | tf_op jit(solution)/shard_map/all_to_all | solution.py:33
  288.2 2.6 fusion
  291.2 1.5 fusion.30
  292.7 7.9 %all-to-all-done.3 = bf16[32,2,2048]{2,1,0:T(2,128)(2,1)S(1)} async-done(((bf16[32,2,2048]{2,1,0:T(2,128)(2,1)}), bf16[32,2,2048]{2,1,0:T(2,128)(2,1)S(1)}, u32[]{:S(2)}, u32[]{:S(2)}) %all-to-all-start.3) | async-done | bytes 262176 | tf_op jit(solution)/shard_map/all_to_all | solution.py:33
  (139 shorter events, 16.6 us)
Async XLA Ops:
  7.2 18.9 %copy-start = (bf16[256,2048]{1,0:T(8,128)(2,1)S(1)}, bf16[256,2048]{1,0:T(8,128)(2,1)}, u32[]{:S(2)}) copy-start(bf16[256,2048]{1,0:T(8,128)(2,1)} %param.10) | copy-start | bytes 3145732
  7.2 117.2 %all-gather.3.cloned.1.call-start = ((), (), s32[]{:S(2)}) async-start(), calls=%async_computation.4 | async-start | bytes 6684672 | tf_op jit(solution)/shard_map/all_gather | solution.py:21
  135.8 5.8 %copy-start.2 = (f32[544,128]{1,0:T(8,128)}, f32[544,128]{1,0:T(8,128)S(1)}, u32[]{:S(2)}) copy-start(f32[544,128]{1,0:T(8,128)S(1)} %fusion.13) | copy-start | bytes 835588
  203.6 13.1 %copy-start.15 = (s32[512]{0:T(512)S(1)}, s32[512]{0:T(512)}, u32[]{:S(2)}) copy-start(s32[512]{0:T(512)} %copy-done.14) | copy-start | bytes 6148
  203.6 13.9 %copy-start.16 = (s32[512,1]{0,1:T(1,128)S(1)}, s32[512,1]{0,1:T(1,128)}, u32[]{:S(2)}) copy-start(s32[512,1]{0,1:T(1,128)} %get-tuple-element.10) | copy-start | bytes 6148
  203.6 30.7 %copy-start.13 = (bf16[31,64]{1,0:T(8,128)(2,1)S(1)}, bf16[31,64]{1,0:T(8,128)(2,1)}, u32[]{:S(2)}) copy-start(bf16[31,64]{1,0:T(8,128)(2,1)} %param.12) | copy-start | bytes 11908
  206.3 22.7 %all-to-all-start.2 = ((bf16[32,17,128]{2,1,0:T(8,128)(2,1)}), bf16[32,17,128]{2,1,0:T(8,128)(2,1)}, u32[]{:S(2)}, u32[]{:S(2)}) async-start(bf16[32,17,128]{2,1,0:T(8,128)(2,1)} %reshape.177), calls=%async_computation.2 | async-start | bytes 393216 | tf_op jit(solution)/shard_map/all_to_all | solution.py:126
  216.6 49.0 %all-gather.5.cloned.1.call-start = ((), (), s32[]{:S(2)}) async-start(), calls=%async_computation.5 | async-start | bytes 1114112 | tf_op jit(solution)/shard_map/all_gather | solution.py:141
  238.4 27.2 %copy-start.12 = (bf16[256,64]{0,1:T(8,128)(2,1)S(1)}, bf16[256,64]{0,1:T(8,128)(2,1)}, u32[]{:S(2)}) copy-start(bf16[256,64]{0,1:T(8,128)(2,1)} %param.11) | copy-start | bytes 98308
  267.9 22.9 %collective-permute-start = (bf16[30,64]{0,1:T(8,128)(2,1)}, bf16[30,64]{0,1:T(8,128)(2,1)S(1)}, u32[]{:S(2)}, u32[]{:S(2)}) collective-permute-start(bf16[30,64]{0,1:T(8,128)(2,1)} %slice.267), channel_id=1, source_target_pairs={{16,0},{32,16},{48,32},{64,48},{80,64},{96,80},{112,96},{128,112},... | collective-permute-start | bytes 11528 | tf_op jit(solution)/shard_map/ppermute | solution.py:40
  276.2 24.3 %all-to-all-start.3 = ((bf16[32,2,2048]{2,1,0:T(2,128)(2,1)}), bf16[32,2,2048]{2,1,0:T(2,128)(2,1)S(1)}, u32[]{:S(2)}, u32[]{:S(2)}) async-start(bf16[32,2,2048]{2,1,0:T(2,128)(2,1)} %reshape.269), calls=%async_computation.3 | async-start | bytes 524288 | tf_op jit(solution)/shard_map/all_to_all | solution.py:33
  287.9 3.0 copy-start.17
  287.9 3.0 copy-start.18
  287.9 3.0 copy-start.19
  287.9 3.0 copy-start.20
  287.9 3.0 copy-start.21
  288.0 3.0 copy-start.22
  288.0 3.0 copy-start.23
  288.0 3.0 copy-start.24
  288.0 3.0 copy-start.25
  288.0 3.0 copy-start.26
  288.0 3.0 copy-start.27
  288.0 3.0 copy-start.28
  288.0 3.0 copy-start.29
  288.0 3.0 copy-start.30
  288.0 3.0 copy-start.31
  288.1 3.0 copy-start.32
  288.1 3.0 copy-start.33
  288.1 3.0 copy-start.34
  288.1 3.0 copy-start.35
  288.1 3.0 copy-start.36
  288.1 3.0 copy-start.37
  (21 other events, 49.3 us)
Sparse Core Ops, SparseCore 0:
  68.6 55.6 all-gather.2
  234.4 31.1 all-gather.4
where the time goes:
time: 310 us; the launch traced here: 309 us
  waiting for transfers between devices  100 us (32%)
  blocking collectives  84 us (27%)
  local copies, waits for them, and re-layouts  46.3 us (15%)
  starting transfers between devices  23.3 us (8%)
  other arithmetic  22.2 us (7%)
  matrix products  17.4 us (6%)
  between operations  14.9 us (5%)
    all_to_all x1, blocking collectives, sum_at_owner(): parts = lax.all_to_all(split_up(shard, dim, peers), axis, 0, 0, tiled=True)  57 us
    all_gather x1, waiting for transfers between devices, sent_together(): whole = lax.all_gather(both, axis, axis=dim, tiled=True)  55.8 us
    all_to_all x1, blocking collectives, in_one_piece(): lax.all_to_all(both, axis, split_axis=split_dim, concat_axis=concat_dim,...  27 us
    all_gather x1, waiting for transfers between devices, body(): mid_grad = lax.all_gather(mid_part, 'tp', axis=1, tiled=True)  25.7 us
    all_to_all x1, starting transfers between devices, sum_at_owner(): parts = lax.all_to_all(split_up(shard, dim, peers), axis, 0, 0, tiled=True)  11.6 us
    all_to_all x1, waiting for transfers between devices, body(): lax.all_to_all(summed.reshape(groups, slot_count, slice_width), 'sp', spl...  11 us
    scatter x1, local copies, waits for them, and re-layouts, body(): send_inputs = jnp.zeros((groups * slot_count, D), jnp.bfloat16).at[slot_i...  10.9 us
    scatter x1, other arithmetic, body(): send_seeds = jnp.zeros((groups * slot_count, D), jnp.bfloat16).at[slot_in...  10.4 us
  transfers between devices with their start and end apart: 5, of which 4 were waited for; matrix products, arithmetic and copies ran while one was open for 6% of the time, Pallas kernels for 0%

commit v1 on v0

v1 whole, which is shorter than its diff:
```python
import functools

import jax
import jax.numpy as jnp
from jax import lax
from jax.experimental import pallas as pl
from jax.experimental.pallas import tpu as pltpu
from jax.sharding import PartitionSpec as P

KERNEL = 31
LANES = 128
MAIN = 16
MESH = pl.DeviceIdType.MESH
F32 = jnp.float32
BF16 = jnp.bfloat16


def silu_slope(value):
    sig = jax.nn.sigmoid(value)
    return sig * (1.0 + value * (1.0 - sig))


def copy_to(src, dst, send, recv, sp, tp):
    return pltpu.make_async_remote_copy(
        src_ref=src,
        dst_ref=dst,
        send_sem=send,
        recv_sem=recv,
        device_id=(sp, tp),
        device_id_type=MESH,
    )


def moe_kernel(
    S,
    T,
    route_e,
    route_w,
    mid,
    cot,
    gate_w,
    up_w,
    down_w,
    grad_gate,
    grad_up,
    grad_down,
    mid_grad,
    send_main,
    send_ext,
    rows,
    ext,
    ext_flat,
    ext_in,
    ext_seed,
    acc_gu,
    acc_h,
    onehot,
    onehot_x,
    hidden,
    pre_grads,
    sib_out,
    sib_in,
    own_part,
    ring_out,
    ring_in,
    back_main,
    back_ext,
    home_main,
    home_ext,
    gathered,
    a2a_send,
    a2a_recv,
    ag_send,
    ag_recv,
    sib_send,
    sib_recv,
    rsib_send,
    rsib_recv,
    rs_send,
    rs_recv,
    ret_send,
    ret_recv,
    mg_send,
    mg_recv,
    mgs_send,
    mgs_recv,
):
    Y = T // 2
    H = Y // 2
    NQ = ag_recv.shape[2]
    KQ = S // NQ
    R = S * MAIN
    N = R + S
    HALF = N // 2
    TOK = mid.shape[0]
    me = lax.axis_index("sp")
    tp = lax.axis_index("tp")
    y = tp // 2
    core = tp % 2
    sib = tp + 1 - 2 * core
    right = lax.rem(tp + 2, T)
    left = lax.rem(tp + T - 2, T)

    def chunk(i, parity):
        return 2 * lax.rem(y - i + 2 * Y, Y) + parity

    barrier = pltpu.get_barrier_semaphore()

    @pl.loop(1, S)
    def _(k):
        pl.semaphore_signal(
            barrier, inc=1, device_id=(lax.rem(me + k, S), tp), device_id_type=MESH
        )

    for peer in (left, right, sib):
        pl.semaphore_signal(barrier, inc=1, device_id=(me, peer), device_id_type=MESH)

    e_rel = route_e[...] - me
    e_rel = jnp.where(e_rel < 0, e_rel + S, e_rel)
    e_iota = lax.broadcasted_iota(jnp.int32, (S, TOK), 0)
    oh = [e_iota == e_rel[k : k + 1, :] for k in range(2)]
    oh_sum = (oh[0] | oh[1]).astype(F32).astype(BF16)
    before = (
        lax.broadcasted_iota(jnp.int32, (TOK, TOK), 0)
        < lax.broadcasted_iota(jnp.int32, (TOK, TOK), 1)
    ).astype(F32).astype(BF16)
    counts = jnp.dot(oh_sum, before, preferred_element_type=F32)
    main_rows = lax.broadcasted_iota(jnp.int32, (R, TOK), 0)
    ext_rows = lax.broadcasted_iota(jnp.int32, (S, TOK), 0)
    pair_rows = lax.broadcasted_iota(jnp.int32, (2 * S, TOK), 0)
    g_main, g_ext, g_pair = [], [], []
    for k in range(2):
        rank = jnp.sum(jnp.where(oh[k], counts, 0.0), axis=0, keepdims=True).astype(jnp.int32)
        own = e_rel[k : k + 1, :]
        key = jnp.where(rank < MAIN, own * MAIN + rank, -1)
        key_x = jnp.where(rank == MAIN, own, -1)
        g_main.append(main_rows == key)
        g_ext.append(ext_rows == key_x)
        g_pair.append(pair_rows == 2 * key_x + 1)
    w = [route_w[k : k + 1, :] for k in range(2)]
    gm = (g_main[0] | g_main[1]).astype(F32).astype(BF16)
    onehot[...] = gm
    onehot_x[...] = (g_ext[0] | g_ext[1]).astype(F32).astype(BF16)
    col = pl.ds(pl.multiple_of(tp * LANES, LANES), LANES)
    mid_c = mid[:, col]
    cot_c = cot[:, col]
    w_main = jnp.sum(
        jnp.where(g_main[0], w[0], 0.0) + jnp.where(g_main[1], w[1], 0.0), axis=1, keepdims=True
    )
    in_rows = jnp.dot(gm, mid_c, preferred_element_type=F32).astype(BF16)
    seed_rows = (w_main * jnp.dot(gm, cot_c, preferred_element_type=F32)).astype(BF16)
    send_main[:, 0:MAIN, :] = in_rows.reshape(S, MAIN, LANES)
    send_main[:, MAIN : 2 * MAIN, :] = seed_rows.reshape(S, MAIN, LANES)
    w_pair = jnp.sum(
        jnp.where(g_pair[0], w[0], 0.0) + jnp.where(g_pair[1], w[1], 0.0), axis=1, keepdims=True
    )
    g_odd = (g_pair[0] | g_pair[1]).astype(F32).astype(BF16)
    pair_even = lax.broadcasted_iota(jnp.int32, (2 * S, S), 0) == 2 * lax.broadcasted_iota(
        jnp.int32, (2 * S, S), 1
    )
    g_even = jnp.dot(
        pair_even.astype(F32).astype(BF16), onehot_x[...], preferred_element_type=F32
    ).astype(BF16)
    pair_val = (
        jnp.dot(g_even, mid_c, preferred_element_type=F32)
        + w_pair * jnp.dot(g_odd, cot_c, preferred_element_type=F32)
    ).astype(BF16)
    for s in range(S):
        send_ext[s] = pair_val[2 * s : 2 * s + 2, :]

    pl.semaphore_wait(barrier, S + 2)

    @pl.loop(1, S)
    def _(k):
        dst = lax.rem(me + k, S)
        q = k // KQ
        copy_to(
            send_main.at[k], rows.at[tp, k], a2a_send.at[0], a2a_recv.at[0, q], dst, tp
        ).start()
        copy_to(
            send_ext.at[k], ext.at[tp, k], a2a_send.at[1], a2a_recv.at[1, q], dst, tp
        ).start()

    rows[tp, 0] = send_main[0]
    ext[tp, 0] = send_ext[0]

    def sub(ref, j, q):
        return ref.at[j, pl.ds(q * KQ, KQ)]

    both = (rows, ext)

    def ag_copies(d, t, q, j):
        peer = right if d == 0 else left
        return [
            copy_to(
                sub(ref, j, q),
                sub(ref, j, q),
                ag_send.at[d, t, q, b],
                ag_recv.at[d, t, q, b],
                me,
                peer,
            )
            for b, ref in enumerate(both)
        ]

    def sib_copies(i, q, j):
        return [
            copy_to(
                sub(ref, j, q),
                sub(ref, j, q),
                sib_send.at[i, q, b],
                sib_recv.at[i, q, b],
                me,
                sib,
            )
            for b, ref in enumerate(both)
        ]

    def carries(d, t, q):
        if t + 1 < H:
            return True
        if t + 1 > H:
            return False
        return (q < NQ // 2) == (d == 0)

    sent = []

    def start_all(copies):
        for c in copies:
            c.start()
        sent.extend(copies)

    for q in range(NQ):
        lo = 1 if q == 0 else q * KQ
        n = (q + 1) * KQ - lo
        if n > 0:
            for b, (src, ref) in enumerate(((send_main, rows), (send_ext, ext))):
                copy_to(
                    src.at[pl.ds(lo, n)],
                    ref.at[tp, pl.ds(lo, n)],
                    a2a_send.at[b],
                    a2a_recv.at[b, q],
                    me,
                    sib,
                ).wait_recv()
        for d in range(2):
            if carries(d, 0, q):
                start_all(ag_copies(d, 0, q, tp))
        start_all(sib_copies(0, q, tp))

    sel_row = lax.broadcasted_iota(jnp.int32, (S, 2 * S), 0)
    sel_col = lax.broadcasted_iota(jnp.int32, (S, 2 * S), 1)
    sels = [(sel_col == 2 * sel_row + b).astype(F32).astype(BF16) for b in range(2)]
    acc_gu[...] = jnp.zeros_like(acc_gu)
    acc_h[...] = jnp.zeros_like(acc_h)

    def in_value(j):
        return jnp.concatenate(
            [rows[j, :, 0:MAIN, :].reshape(R, LANES), ext_in[j]], axis=0
        )

    def seed_value(j):
        return jnp.concatenate(
            [rows[j, :, MAIN : 2 * MAIN, :].reshape(R, LANES), ext_seed[j]], axis=0
        )

    def use_pair(i):
        for q in range(NQ):
            for c in sib_copies(i, q, chunk(i, 1 - core)):
                c.wait_recv()
        j0 = chunk(i, 0)
        for p in range(2):
            j = j0 + p
            for s in range(S):
                ext_flat[2 * s : 2 * s + 2, :] = ext[j, s]
            flat = ext_flat[...]
            ext_in[j] = jnp.dot(sels[0], flat, preferred_element_type=F32).astype(BF16)
            ext_seed[j] = jnp.dot(sels[1], flat, preferred_element_type=F32).astype(BF16)
        span = pl.ds(pl.multiple_of(j0 * LANES, 2 * LANES), 2 * LANES)
        w_gu = jnp.concatenate([gate_w[span, :], up_w[span, :]], axis=1)
        x = jnp.concatenate([in_value(j0), in_value(j0 + 1)], axis=1)
        acc_gu[...] += jnp.dot(x, w_gu, preferred_element_type=F32)
        g = jnp.concatenate([seed_value(j0), seed_value(j0 + 1)], axis=1)
        acc_h[...] += lax.dot_general(
            g, down_w[:, span], (((1,), (1,)), ((), ())), preferred_element_type=F32
        )

    use_pair(0)
    for t in range(H):
        for q in range(NQ):
            for d in range(2):
                if not carries(d, t, q):
                    continue
                i = t + 1 if d == 0 else Y - (t + 1)
                j = chunk(i, core)
                for c in ag_copies(d, t, q, j):
                    c.wait_recv()
                if carries(d, t + 1, q):
                    start_all(ag_copies(d, t + 1, q, j))
                start_all(sib_copies(i, q, j))
        if t + 1 < H:
            use_pair(t + 1)
            use_pair(Y - (t + 1))
        else:
            use_pair(H)

    gate_pre = acc_gu[:, 0:LANES]
    up_pre = acc_gu[:, LANES : 2 * LANES]
    h_grad = acc_h[...]
    sig = jax.nn.sigmoid(gate_pre)
    act = gate_pre * sig
    hidden[...] = (act * up_pre).astype(BF16)
    pre_grads[:, 0:LANES] = (
        h_grad * up_pre * (sig * (1.0 + gate_pre * (1.0 - sig)))
    ).astype(BF16)
    pre_grads[:, LANES : 2 * LANES] = (h_grad * act).astype(BF16)

    def partial(j):
        span = pl.ds(pl.multiple_of(j * LANES, LANES), LANES)
        w_gu = jnp.concatenate([gate_w[span, :], up_w[span, :]], axis=1)
        return lax.dot_general(
            pre_grads[...], w_gu, (((1,), (1,)), ((), ())), preferred_element_type=F32
        )

    order = [H] + [o for d in range(H - 1, 0, -1) for o in (d, Y - d)] + [0]
    if H == 0:
        order = [0]

    def dest(o, parity):
        return 2 * lax.rem(y + o, Y) + parity

    def rsib_copy(o):
        return copy_to(
            sib_out.at[o], sib_in.at[o], rsib_send.at[o], rsib_recv.at[o], me, sib
        )

    for o in order:
        sib_out[o] = partial(dest(o, 1 - core)).astype(BF16)
        start_all([rsib_copy(o)])

    def weight_grads(j):
        span = pl.ds(pl.multiple_of(j * LANES, LANES), LANES)
        both_g = lax.dot_general(
            in_value(j), pre_grads[...], (((0,), (0,)), ((), ())), preferred_element_type=F32
        ).astype(BF16)
        grad_gate[span, :] = both_g[:, 0:LANES]
        grad_up[span, :] = both_g[:, LANES : 2 * LANES]
        grad_down[:, span] = lax.dot_general(
            hidden[...], seed_value(j), (((0,), (0,)), ((), ())), preferred_element_type=F32
        ).astype(BF16)

    for o in order:
        own_part[o] = partial(dest(o, core))

    def half(h):
        return pl.ds(h * HALF, HALF)

    def rs_copy(d, t, h):
        return copy_to(
            ring_out.at[d, t, h],
            ring_in.at[d, t, h],
            rs_send.at[d, t, h],
            rs_recv.at[d, t, h],
            me,
            right if d == 0 else left,
        )

    def rs_has(d, t, h):
        if t < 0:
            return False
        return t > 0 or h == d

    done = 0
    for t in range(H):
        dist = H - t
        for h in range(2):
            for d in range(2):
                if not rs_has(d, t, h):
                    continue
                o = dist if d == 0 else Y - dist
                if (d == 0 or dist < H) and h == (d if t == 0 else 0):
                    rsib_copy(o).wait_recv()
                value = own_part[o, half(h), :] + sib_in[o, half(h), :].astype(F32)
                if rs_has(d, t - 1, h):
                    rs_copy(d, t - 1, h).wait_recv()
                    value = value + ring_in[d, t - 1, h].astype(F32)
                ring_out[d, t, h] = value.astype(BF16)
                start_all([rs_copy(d, t, h)])
        stop = T * (t + 1) // H

        @pl.loop(done, stop)
        def _(j):
            weight_grads(j)

        done = stop

    rsib_copy(0).wait_recv()
    for h in range(2):
        value = own_part[0, half(h), :] + sib_in[0, half(h), :].astype(F32)
        for d in range(2):
            if rs_has(d, H - 1, h):
                rs_copy(d, H - 1, h).wait_recv()
                value = value + ring_in[d, H - 1, h].astype(F32)
        own_part[0, half(h), :] = value
    back_main[...] = own_part[0, 0:R, :].astype(BF16).reshape(S, MAIN, LANES)
    last = own_part[0, R:N, :].astype(BF16).astype(F32)
    for s in range(S):
        back_ext[s] = last[s : s + 1, :]

    @pl.loop(1, S)
    def _(k):
        dst = lax.rem(me + S - k, S)
        copy_to(
            back_main.at[k], home_main.at[k], ret_send.at[0], ret_recv.at[0], dst, tp
        ).start()
        copy_to(
            back_ext.at[k], home_ext.at[k], ret_send.at[1], ret_recv.at[1], dst, tp
        ).start()

    home_main[0] = back_main[0]
    home_ext[0] = back_ext[0]
    if S > 1:
        for b, (src, ref) in enumerate(((back_main, home_main), (back_ext, home_ext))):
            copy_to(
                src.at[pl.ds(1, S - 1)],
                ref.at[pl.ds(1, S - 1)],
                ret_send.at[b],
                ret_recv.at[b],
                me,
                sib,
            ).wait()
        for b, (src, ref) in enumerate(((send_main, rows), (send_ext, ext))):
            copy_to(
                src.at[pl.ds(1, S - 1)],
                ref.at[tp, pl.ds(1, S - 1)],
                a2a_send.at[b],
                a2a_recv.at[b, 0],
                me,
                sib,
            ).wait_send()
    home_x = jnp.concatenate([home_ext[s] for s in range(S)], axis=0).astype(BF16)
    moe = lax.dot_general(
        onehot[...],
        home_main[...].reshape(R, LANES),
        (((0,), (0,)), ((), ())),
        preferred_element_type=F32,
    ) + lax.dot_general(
        onehot_x[...], home_x, (((0,), (0,)), ((), ())), preferred_element_type=F32
    )
    gathered[tp] = (cot[:, col].astype(F32) + moe).astype(BF16)

    TH = TOK // 2

    def mg_copy(d, t, h, j):
        part = gathered.at[j, pl.ds(h * TH, TH)]
        return copy_to(
            part,
            part,
            mg_send.at[d, t, h],
            mg_recv.at[d, t, h],
            me,
            right if d == 0 else left,
        )

    def mgs_copy(i, h, j):
        part = gathered.at[j, pl.ds(h * TH, TH)]
        return copy_to(part, part, mgs_send.at[i, h], mgs_recv.at[i, h], me, sib)

    def mg_carries(d, t, h):
        if t + 1 < H:
            return True
        if t + 1 > H:
            return False
        return h == d

    for h in range(2):
        for d in range(2):
            if mg_carries(d, 0, h):
                start_all([mg_copy(d, 0, h, tp)])
        start_all([mgs_copy(0, h, tp)])
    for t in range(H):
        for h in range(2):
            for d in range(2):
                if not mg_carries(d, t, h):
                    continue
                i = t + 1 if d == 0 else Y - (t + 1)
                j = chunk(i, core)
                mg_copy(d, t, h, j).wait_recv()
                if mg_carries(d, t + 1, h):
                    start_all([mg_copy(d, t + 1, h, j)])
                start_all([mgs_copy(i, h, j)])
    for i in range(Y):
        for h in range(2):
            mgs_copy(i, h, chunk(i, 1 - core)).wait_recv()
    for j in range(T):
        mid_grad[:, j * LANES : (j + 1) * LANES] = gathered[j]
    for c in sent:
        c.wait_send()


def moe_call(S, T, route_e, route_w, mid, cot, gate_w, up_w, down_w):
    Y = T // 2
    H = Y // 2
    TOK, D = mid.shape
    NQ = min(4, S)
    R = S * MAIN
    N = R + S
    vmem = pl.BlockSpec(memory_space=pltpu.VMEM)
    dma = pltpu.SemaphoreType.DMA
    scratch = [
        pltpu.VMEM((S, 2 * MAIN, LANES), BF16),
        pltpu.VMEM((S, 2, LANES), BF16),
        pltpu.VMEM((T, S, 2 * MAIN, LANES), BF16),
        pltpu.VMEM((T, S, 2, LANES), BF16),
        pltpu.VMEM((2 * S, LANES), BF16),
        pltpu.VMEM((T, S, LANES), BF16),
        pltpu.VMEM((T, S, LANES), BF16),
        pltpu.VMEM((N, 2 * LANES), F32),
        pltpu.VMEM((N, LANES), F32),
        pltpu.VMEM((R, TOK), BF16),
        pltpu.VMEM((S, TOK), BF16),
        pltpu.VMEM((N, LANES), BF16),
        pltpu.VMEM((N, 2 * LANES), BF16),
        pltpu.VMEM((Y, N, LANES), BF16),
        pltpu.VMEM((Y, N, LANES), BF16),
        pltpu.VMEM((Y, N, LANES), F32),
        pltpu.VMEM((2, H, 2, N // 2, LANES), BF16),
        pltpu.VMEM((2, H, 2, N // 2, LANES), BF16),
        pltpu.VMEM((S, MAIN, LANES), BF16),
        pltpu.VMEM((S, 1, LANES), F32),
        pltpu.VMEM((S, MAIN, LANES), BF16),
        pltpu.VMEM((S, 1, LANES), F32),
        pltpu.VMEM((T, TOK, LANES), BF16),
        dma((2,)),
        dma((2, NQ)),
        dma((2, H, NQ, 2)),
        dma((2, H, NQ, 2)),
        dma((Y, NQ, 2)),
        dma((Y, NQ, 2)),
        dma((Y,)),
        dma((Y,)),
        dma((2, H, 2)),
        dma((2, H, 2)),
        dma((2,)),
        dma((2,)),
        dma((2, H, 2)),
        dma((2, H, 2)),
        dma((Y, 2)),
        dma((Y, 2)),
    ]
    return pl.pallas_call(
        functools.partial(moe_kernel, S, T),
        out_shape=(
            jax.ShapeDtypeStruct((D, LANES), BF16),
            jax.ShapeDtypeStruct((D, LANES), BF16),
            jax.ShapeDtypeStruct((LANES, D), BF16),
            jax.ShapeDtypeStruct((TOK, D), BF16),
        ),
        in_specs=[vmem] * 7,
        out_specs=(vmem,) * 4,
        scratch_shapes=scratch,
        compiler_params=pltpu.CompilerParams(
            collective_id=0, has_side_effects=True, vmem_limit_bytes=60 * 1024 * 1024
        ),
    )(route_e, route_w, mid, cot, gate_w, up_w, down_w)


def split_up(shard, dim, peers):
    shape = shard.shape
    parts = shard.reshape(*shape[:dim], peers, shape[dim] // peers, *shape[dim + 1 :])
    return jnp.moveaxis(parts, dim, 0)


def sum_at_owner(shard, axis, dim):
    peers = lax.axis_size(axis)
    parts = lax.all_to_all(split_up(shard, dim, peers), axis, 0, 0, tiled=True)
    return jnp.sum(parts.astype(jnp.float32), axis=0)


def passed_along(value, axis, steps):
    count = lax.axis_size(axis)
    initial, last = (max(0, -steps), min(count, count - steps))
    return lax.ppermute(value, axis, [(source, source + steps) for source in range(initial, last)])


def body(
    S,
    T,
    mid_state,
    conv_pre,
    conv_taps,
    out_proj,
    route_expert,
    route_weight,
    gate_w,
    up_w,
    down_w,
    cotangent,
):
    token_count = mid_state.shape[0]
    grad_gate, grad_up, grad_down, mid_grad = moe_call(
        S,
        T,
        route_expert.T,
        route_weight.T,
        mid_state,
        cotangent,
        gate_w[0],
        up_w[0],
        down_w[0],
    )
    pre_float = conv_pre.astype(jnp.float32)
    activated = jax.nn.silu(pre_float).astype(jnp.bfloat16)
    mixed_grad = lax.dot_general(
        mid_grad, out_proj, (((1,), (1,)), ((), ())), preferred_element_type=jnp.float32
    )
    conv_grad = (mixed_grad * silu_slope(pre_float)).astype(jnp.bfloat16)
    next_head = passed_along(conv_grad[: KERNEL - 1], "sp", -1)
    extended = jnp.concatenate([conv_grad, next_head], axis=0).astype(jnp.float32)
    conv_input_grad = jnp.zeros(conv_grad.shape, jnp.float32)
    for lag_index in range(KERNEL):
        conv_input_grad = (
            conv_input_grad
            + conv_taps[lag_index].astype(jnp.float32)[None, :]
            * extended[lag_index : lag_index + token_count]
        )
    grad_proj = sum_at_owner(
        lax.dot_general(
            mid_grad, activated, (((0,), (0,)), ((), ())), preferred_element_type=jnp.float32
        ).astype(jnp.bfloat16),
        "sp",
        0,
    )
    return (grad_gate[None], grad_up[None], grad_down[None], grad_proj, conv_input_grad)


def solution(mesh):
    placed = (
        P("sp", None),
        P("sp", "tp"),
        P(None, "tp"),
        P("tp", None),
        P("sp", None),
        P("sp", None),
        P("sp", None, "tp"),
        P("sp", None, "tp"),
        P("sp", "tp", None),
        P("sp", None),
    )
    return jax.shard_map(
        functools.partial(body, mesh.shape["sp"], mesh.shape["tp"]),
        mesh=mesh,
        in_specs=placed,
        out_specs=(
            P("sp", None, "tp"),
            P("sp", None, "tp"),
            P("sp", "tp", None),
            P("sp", "tp"),
            P("sp", "tp"),
        ),
        check_vma=False,
    )
```

time: 310 us -> 128 us (0.41)
  Pallas kernels: 0 us -> 95 us
  waiting for transfers between devices: 100 us -> 12.2 us
  blocking collectives: 84 us -> 0 us
  local copies, waits for them, and re-layouts: 46.3 us -> 6.16 us
  other arithmetic: 22.2 us -> 1.67 us
  matrix products: 17.4 us -> 2.04 us
  between operations: 14.9 us -> 0.79 us
  starting transfers between devices: 23.3 us -> 9.35 us
    pallas_call x0 -> x1, Pallas kernels: none -> 95 us  [moe_call(): pl.pallas_call(functools.partial(moe_kernel, S, T), out_shape=(jax.ShapeD...]
    all_to_all x2 -> x0, blocking collectives: 84 us -> none  [the longest x1 57 us: sum_at_owner(): parts = lax.all_to_all(split_up(shard, dim, peers), axis, 0, 0, tiled=True)]
    all_gather x2 -> x0, waiting for transfers between devices: 81.6 us -> none  [the longest x1 55.8 us: sent_together(): whole = lax.all_gather(both, axis, axis=dim, tiled=True)]
    dot_general x8 -> x0, matrix products: 14.2 us -> none  [the longest x1 2.77 us: body(): lax.dot_general(inputs, up_grad, (((0,), (0,)), ((), ())), preferred_elem...]
    reshape x6 -> x0, local copies, waits for them, and re-layouts: 14.1 us -> none  [the longest x1 4.36 us: body(): seeds = got_seeds.reshape(groups * slot_count, D)]
    all_to_all x1 -> x0, waiting for transfers between devices: 11 us -> none  [body(): lax.all_to_all(summed.reshape(groups, slot_count, slice_width), 'sp', spl...]
    scatter x1 -> x0, local copies, waits for them, and re-layouts: 10.9 us -> none  [body(): send_inputs = jnp.zeros((groups * slot_count, D), jnp.bfloat16).at[slot_i...]
    scatter x1 -> x0, other arithmetic: 10.4 us -> none  [body(): send_seeds = jnp.zeros((groups * slot_count, D), jnp.bfloat16).at[slot_in...]
  transfers between devices with their start and end apart: 5 -> 2, of which waited for: 4 -> 1; matrix products, arithmetic and copies ran while one was open for 6% -> 3% of each run, Pallas kernels for 0% -> 0%
where the time goes in v1:
time: 128 us; the launch traced here: 127 us
  Pallas kernels  95 us (74%)
  waiting for transfers between devices  12.2 us (10%)
  starting transfers between devices  9.35 us (7%)
  local copies, waits for them, and re-layouts  6.16 us (5%)
  matrix products  2.04 us (2%)
  other arithmetic  1.67 us (1%)
    pallas_call x1, Pallas kernels, moe_call(): pl.pallas_call(functools.partial(moe_kernel, S, T), out_shape=(jax.ShapeD...  95 us
    all_to_all x1, waiting for transfers between devices, sum_at_owner(): parts = lax.all_to_all(split_up(shard, dim, peers), axis, 0, 0, tiled=True)  12.2 us
    all_to_all x1, starting transfers between devices, sum_at_owner(): parts = lax.all_to_all(split_up(shard, dim, peers), axis, 0, 0, tiled=True)  8.06 us
    unnamed x20, local copies, waits for them, and re-layouts  5.44 us
  transfers between devices with their start and end apart: 2, of which 1 were waited for; matrix products, arithmetic and copies ran while one was open for 3% of the time, Pallas kernels for 0%

profile of v1, /device:TPU:8, one launch (start us, length us, event | category | flops | bytes accessed | tf_op | source)
XLA Modules:
  0.0 127.3 jit_solution(7458351549397220760)
XLA Ops:
  0.6 0.0 copy-start
  0.6 0.0 copy-start.5
  0.7 95.0 %shard_map.137 = (bf16[2048,128]{1,0:T(8,128)(2,1)}, bf16[2048,128]{1,0:T(8,128)(2,1)}, bf16[128,2048]{1,0:T(8,128)(2,1)}, bf16[256,2048]{1,0:T(8,128)(2,1)}) custom-call(s32[2,256]{1,0:T(2,128)} %bitcast.118, f32[2,256]{1,0:T(2,128)} %bitcast.119, bf16[256,2048]{1,0:T(8,128)(2,1)} %mid.1, bf16[256,2048]{1,0:T(8,128)(2,1)} %cot.1, ...), custom_call_target="tpu_custom_call" | custom-call | tf_op jit(solution)/shard_map/pallas_call | solution.py:551
  95.7 0.0 copy-start.1
  95.7 0.0 copy-done
  95.7 0.0 copy-done.5
  95.7 1.8 %fusion = bf16[256,64]{0,1:T(8,128)(2,1)S(1)} fusion(bf16[256,2048]{1,0:T(8,128)(2,1)} %get-tuple-element.12, bf16[64,2048]{1,0:T(8,128)(2,1)S(1)} %copy-done, bf16[256,64]{0,1:T(8,128)(2,1)S(1)} %copy-done.5), kind=kOutput, calls=%fused_computation.2 | convolution fusion | flops 67272704 | bytes 1376256 | tf_op jit(solution)/shard_map/dot_general | solution.py:614
  97.5 1.3 %collective-permute-start = (bf16[30,64]{0,1:T(8,128)(2,1)S(1)}, bf16[30,64]{0,1:T(8,128)(2,1)S(1)}, u32[]{:S(2)}, u32[]{:S(2)}) collective-permute-start(bf16[30,64]{0,1:T(8,128)(2,1)S(1)} %slice.252), channel_id=1, source_target_pairs={{16,0},{32,16},{48,32},{64,48},{80,64},{96,80},{112,96},{128,112},... | collective-permute-start | bytes 11528 | tf_op jit(solution)/shard_map/ppermute | solution.py:583
  98.8 0.0 copy-done.1
  98.8 0.3 convolution_convert_fusion
  99.1 0.5 reshape.13
  99.6 0.2 copy.20
  99.8 1.1 reshape.45
  100.9 0.0 copy-start.6
  100.9 8.1 %all-to-all-start = ((bf16[32,2,2048]{2,1,0:T(2,128)(2,1)}), bf16[32,2,2048]{2,1,0:T(2,128)(2,1)S(1)}, u32[]{:S(2)}, u32[]{:S(2)}) async-start(bf16[32,2,2048]{2,1,0:T(2,128)(2,1)} %reshape.45), calls=%async_computation | async-start | bytes 524288 | tf_op jit(solution)/shard_map/all_to_all | solution.py:576
  109.0 0.0 copy-done.6
  109.1 0.0 collective-permute-done
  109.1 1.5 %fusion.7 = f32[256,64]{0,1:T(8,128)} fusion(f32[286,64]{0,1:T(8,128)S(1)} %maximum_convert_fusion, f32[64]{0:T(128)S(1)} %get-tuple-element.47, f32[64]{0:T(128)S(1)} %get-tuple-element.48, f32[64]{0:T(128)S(1)} %get-tuple-element.19, f32[64]{0:T(128)S(1)} %get-tuple-element.20, f32[64]{0:T(128)S(1)} %get-tuple-element.21, f32[64]{0:T(128)S(1)} %get-tuple-element.22, ...), kind=kLoop, calls=%fused_computation.14 | loop fusion | flops 999424 | bytes 2105088 | tf_op jit(solution)/shard_map/add | solution.py:623
  110.6 0.0 copy-start.4
  110.6 12.2 %all-to-all-done = bf16[32,2,2048]{2,1,0:T(2,128)(2,1)S(1)} async-done(((bf16[32,2,2048]{2,1,0:T(2,128)(2,1)}), bf16[32,2,2048]{2,1,0:T(2,128)(2,1)S(1)}, u32[]{:S(2)}, u32[]{:S(2)}) %all-to-all-start) | async-done | bytes 262176 | tf_op jit(solution)/shard_map/all_to_all | solution.py:576
  122.8 0.4 reshape.46
  123.2 0.1 convert_reduce_fusion
  123.3 0.7 copy.17
  124.0 0.0 copy-done.4
  124.0 0.0 copy-start.3
  124.0 0.8 copy.24
  124.8 0.4 copy-done.3
  125.3 0.0 copy-start.2
  125.3 0.8 copy.25
  126.1 0.4 copy-done.2
  126.5 0.8 copy.26
  (4 shorter events, 0.0 us)
Async XLA Ops:
  0.6 95.1 %copy-start = (bf16[64,2048]{1,0:T(8,128)(2,1)S(1)}, bf16[64,2048]{1,0:T(8,128)(2,1)}, u32[]{:S(2)}) copy-start(bf16[64,2048]{1,0:T(8,128)(2,1)} %param.13) | copy-start | bytes 786436
  0.6 95.1 %copy-start.5 = (bf16[256,64]{0,1:T(8,128)(2,1)S(1)}, bf16[256,64]{0,1:T(8,128)(2,1)}, u32[]{:S(2)}) copy-start(bf16[256,64]{0,1:T(8,128)(2,1)} %param.11) | copy-start | bytes 98308
  95.7 3.1 %copy-start.1 = (bf16[256,2048]{1,0:T(8,128)(2,1)S(1)}, bf16[256,2048]{1,0:T(8,128)(2,1)}, u32[]{:S(2)}) copy-start(bf16[256,2048]{1,0:T(8,128)(2,1)} %get-tuple-element.12) | copy-start | bytes 3145732
  97.5 11.6 %collective-permute-start = (bf16[30,64]{0,1:T(8,128)(2,1)S(1)}, bf16[30,64]{0,1:T(8,128)(2,1)S(1)}, u32[]{:S(2)}, u32[]{:S(2)}) collective-permute-start(bf16[30,64]{0,1:T(8,128)(2,1)S(1)} %slice.252), channel_id=1, source_target_pairs={{16,0},{32,16},{48,32},{64,48},{80,64},{96,80},{112,96},{128,112},... | collective-permute-start | bytes 11528 | tf_op jit(solution)/shard_map/ppermute | solution.py:583
  100.9 8.1 %copy-start.6 = (bf16[31,64]{1,0:T(8,128)(2,1)S(1)}, bf16[31,64]{1,0:T(8,128)(2,1)}, u32[]{:S(2)}) copy-start(bf16[31,64]{1,0:T(8,128)(2,1)} %param.12) | copy-start | bytes 11908
  100.9 21.9 %all-to-all-start = ((bf16[32,2,2048]{2,1,0:T(2,128)(2,1)}), bf16[32,2,2048]{2,1,0:T(2,128)(2,1)S(1)}, u32[]{:S(2)}, u32[]{:S(2)}) async-start(bf16[32,2,2048]{2,1,0:T(2,128)(2,1)} %reshape.45), calls=%async_computation | async-start | bytes 524288 | tf_op jit(solution)/shard_map/all_to_all | solution.py:576
  110.6 13.4 %copy-start.4 = (bf16[2048,128]{1,0:T(8,128)(2,1)S(1)}, bf16[2048,128]{1,0:T(8,128)(2,1)}, u32[]{:S(2)}) copy-start(bf16[2048,128]{1,0:T(8,128)(2,1)} %get-tuple-element.9) | copy-start | bytes 1572868
  124.0 1.2 copy-start.3
  125.3 1.2 copy-start.2

commit v2 on v1

--- a/solution.py
+++ b/solution.py
@@ -13,11 +13,6 @@
 MESH = pl.DeviceIdType.MESH
 F32 = jnp.float32
 BF16 = jnp.bfloat16
-
-
-def silu_slope(value):
-    sig = jax.nn.sigmoid(value)
-    return sig * (1.0 + value * (1.0 - sig))
 
 
 def copy_to(src, dst, send, recv, sp, tp):
@@ -41,10 +36,14 @@
     gate_w,
     up_w,
     down_w,
+    conv_pre,
+    conv_taps,
+    out_proj,
     grad_gate,
     grad_up,
     grad_down,
-    mid_grad,
+    grad_proj,
+    conv_in_grad,
     send_main,
     send_ext,
     rows,
@@ -68,6 +67,11 @@
     home_main,
     home_ext,
     gathered,
+    mixed,
+    proj_out,
+    proj_in,
+    halo_out,
+    halo_in,
     a2a_send,
     a2a_recv,
     ag_send,
@@ -84,6 +88,10 @@
     mg_recv,
     mgs_send,
     mgs_recv,
+    proj_send,
+    proj_recv,
+    halo_send,
+    halo_recv,
 ):
     Y = T // 2
     H = Y // 2
@@ -93,6 +101,8 @@
     N = R + S
     HALF = N // 2
     TOK = mid.shape[0]
+    CC = conv_pre.shape[0]
+    HW = halo_out.shape[1]
     me = lax.axis_index("sp")
     tp = lax.axis_index("tp")
     y = tp // 2
@@ -473,11 +483,39 @@
             return False
         return h == d
 
+    pre = conv_pre[...].astype(F32)
+    pre_sig = jax.nn.sigmoid(pre)
+    activated = (pre * pre_sig).astype(BF16)
+    mixed[...] = jnp.zeros_like(mixed)
+    units = proj_out.shape[0] // S
+    low = lax.broadcasted_iota(jnp.int32, (CC // 2, LANES), 1) < LANES // 2
+
+    def use_mid(i):
+        for h in range(2):
+            mgs_copy(i, h, chunk(i, 1 - core)).wait_recv()
+        j0 = chunk(i, 0)
+        span = pl.ds(pl.multiple_of(j0 * LANES, 2 * LANES), 2 * LANES)
+        g = jnp.concatenate([gathered[j0], gathered[j0 + 1]], axis=1)
+        mixed[...] += lax.dot_general(
+            out_proj[:, span], g, (((1,), (1,)), ((), ())), preferred_element_type=F32
+        )
+        part = jnp.dot(activated, g, preferred_element_type=F32)
+        for p in range(2):
+            top = part[0 : CC // 2, p * LANES : (p + 1) * LANES]
+            low_c = part[CC // 2 : CC, p * LANES : (p + 1) * LANES]
+            proj_out[2 * (j0 + p)] = jnp.where(
+                low, top, pltpu.roll(low_c, LANES // 2, 1)
+            ).astype(BF16)
+            proj_out[2 * (j0 + p) + 1] = jnp.where(
+                low, pltpu.roll(top, LANES // 2, 1), low_c
+            ).astype(BF16)
+
     for h in range(2):
         for d in range(2):
             if mg_carries(d, 0, h):
                 start_all([mg_copy(d, 0, h, tp)])
         start_all([mgs_copy(0, h, tp)])
+    use_mid(0)
     for t in range(H):
         for h in range(2):
             for d in range(2):
@@ -489,19 +527,70 @@
                 if mg_carries(d, t + 1, h):
                     start_all([mg_copy(d, t + 1, h, j)])
                 start_all([mgs_copy(i, h, j)])
-    for i in range(Y):
-        for h in range(2):
-            mgs_copy(i, h, chunk(i, 1 - core)).wait_recv()
-    for j in range(T):
-        mid_grad[:, j * LANES : (j + 1) * LANES] = gathered[j]
+        if t + 1 < H:
+            use_mid(t + 1)
+            use_mid(Y - (t + 1))
+        else:
+            use_mid(H)
+
+    conv_grad = (mixed[...] * (pre_sig * (1.0 + pre * (1.0 - pre_sig)))).astype(BF16)
+    halo_out[...] = conv_grad[:, 0:HW]
+    halo = copy_to(
+        halo_out, halo_in, halo_send.at[0], halo_recv.at[0], lax.rem(me + S - 1, S), tp
+    )
+    if S > 1:
+        start_all([halo])
+
+    def block(ref, n):
+        return ref.at[pl.ds(n * units, units)]
+
+    @pl.loop(1, S)
+    def _(k):
+        dst = lax.rem(me + k, S)
+        copy_to(
+            block(proj_out, dst), block(proj_in, k), proj_send.at[0], proj_recv.at[0], dst, tp
+        ).start()
+
+    eye = (
+        lax.broadcasted_iota(jnp.int32, (KERNEL, KERNEL), 0)
+        == lax.broadcasted_iota(jnp.int32, (KERNEL, KERNEL), 1)
+    ).astype(F32).astype(BF16)
+    taps = lax.dot_general(
+        conv_taps[...], eye, (((0,), (0,)), ((), ())), preferred_element_type=F32
+    )
+    halo.wait_recv()
+    beyond = jnp.where(me == S - 1, 0.0, halo_in[...].astype(F32))
+    extended = jnp.concatenate([conv_grad.astype(F32), beyond], axis=1)
+    total = taps[:, 0:1] * extended[:, 0:TOK]
+    for lag in range(1, KERNEL):
+        shifted = pltpu.roll(extended, TOK + HW - lag, 1)
+        total = total + taps[:, lag : lag + 1] * shifted[:, 0:TOK]
+    conv_in_grad[...] = total
+
+    if S > 1:
+        copy_to(
+            proj_out.at[pl.ds(units, (S - 1) * units)],
+            proj_in.at[pl.ds(units, (S - 1) * units)],
+            proj_send.at[0],
+            proj_recv.at[0],
+            me,
+            sib,
+        ).wait()
+    for u in range(units):
+        z = proj_out[me * units + u].astype(F32)
+        for k in range(1, S):
+            z = z + proj_in[k * units + u].astype(F32)
+        tall = jnp.concatenate([z, pltpu.roll(z, LANES // 2, 1)], axis=0)
+        grad_proj[u * (LANES // 2) : (u + 1) * (LANES // 2), :] = tall.T[0 : LANES // 2, :]
     for c in sent:
         c.wait_send()
 
 
-def moe_call(S, T, route_e, route_w, mid, cot, gate_w, up_w, down_w):
+def moe_call(S, T, *args):
     Y = T // 2
     H = Y // 2
-    TOK, D = mid.shape
+    TOK, D = args[2].shape
+    CC = args[7].shape[0]
     NQ = min(4, S)
     R = S * MAIN
     N = R + S
@@ -531,6 +620,11 @@
         pltpu.VMEM((S, MAIN, LANES), BF16),
         pltpu.VMEM((S, 1, LANES), F32),
         pltpu.VMEM((T, TOK, LANES), BF16),
+        pltpu.VMEM((CC, TOK), F32),
+        pltpu.VMEM((2 * T, CC // 2, LANES), BF16),
+        pltpu.VMEM((2 * T, CC // 2, LANES), BF16),
+        pltpu.VMEM((CC, min(LANES, TOK)), BF16),
+        pltpu.VMEM((CC, min(LANES, TOK)), BF16),
         dma((2,)),
         dma((2, NQ)),
         dma((2, H, NQ, 2)),
@@ -547,6 +641,10 @@
         dma((2, H, 2)),
         dma((Y, 2)),
         dma((Y, 2)),
+        dma((1,)),
+        dma((1,)),
+        dma((1,)),
+        dma((1,)),
     ]
     return pl.pallas_call(
         functools.partial(moe_kernel, S, T),
@@ -554,33 +652,16 @@
             jax.ShapeDtypeStruct((D, LANES), BF16),
             jax.ShapeDtypeStruct((D, LANES), BF16),
             jax.ShapeDtypeStruct((LANES, D), BF16),
-            jax.ShapeDtypeStruct((TOK, D), BF16),
+            jax.ShapeDtypeStruct((D // S, CC), F32),
+            jax.ShapeDtypeStruct((CC, TOK), F32),
         ),
-        in_specs=[vmem] * 7,
-        out_specs=(vmem,) * 4,
+        in_specs=[vmem] * len(args),
+        out_specs=(vmem,) * 5,
         scratch_shapes=scratch,
         compiler_params=pltpu.CompilerParams(
             collective_id=0, has_side_effects=True, vmem_limit_bytes=60 * 1024 * 1024
         ),
-    )(route_e, route_w, mid, cot, gate_w, up_w, down_w)
-
-
-def split_up(shard, dim, peers):
-    shape = shard.shape
-    parts = shard.reshape(*shape[:dim], peers, shape[dim] // peers, *shape[dim + 1 :])
-    return jnp.moveaxis(parts, dim, 0)
-
-
-def sum_at_owner(shard, axis, dim):
-    peers = lax.axis_size(axis)
-    parts = lax.all_to_all(split_up(shard, dim, peers), axis, 0, 0, tiled=True)
-    return jnp.sum(parts.astype(jnp.float32), axis=0)
-
-
-def passed_along(value, axis, steps):
-    count = lax.axis_size(axis)
-    initial, last = (max(0, -steps), min(count, count - steps))
-    return lax.ppermute(value, axis, [(source, source + steps) for source in range(initial, last)])
+    )(*args)
 
 
 def body(
@@ -597,8 +678,7 @@
     down_w,
     cotangent,
 ):
-    token_count = mid_state.shape[0]
-    grad_gate, grad_up, grad_down, mid_grad = moe_call(
+    grad_gate, grad_up, grad_down, grad_proj, conv_in_grad = moe_call(
         S,
         T,
         route_expert.T,
@@ -608,30 +688,11 @@
         gate_w[0],
         up_w[0],
         down_w[0],
-    )
-    pre_float = conv_pre.astype(jnp.float32)
-    activated = jax.nn.silu(pre_float).astype(jnp.bfloat16)
-    mixed_grad = lax.dot_general(
-        mid_grad, out_proj, (((1,), (1,)), ((), ())), preferred_element_type=jnp.float32
-    )
-    conv_grad = (mixed_grad * silu_slope(pre_float)).astype(jnp.bfloat16)
-    next_head = passed_along(conv_grad[: KERNEL - 1], "sp", -1)
-    extended = jnp.concatenate([conv_grad, next_head], axis=0).astype(jnp.float32)
-    conv_input_grad = jnp.zeros(conv_grad.shape, jnp.float32)
-    for lag_index in range(KERNEL):
-        conv_input_grad = (
-            conv_input_grad
-            + conv_taps[lag_index].astype(jnp.float32)[None, :]
-            * extended[lag_index : lag_index + token_count]
-        )
-    grad_proj = sum_at_owner(
-        lax.dot_general(
-            mid_grad, activated, (((0,), (0,)), ((), ())), preferred_element_type=jnp.float32
-        ).astype(jnp.bfloat16),
-        "sp",
-        0,
-    )
-    return (grad_gate[None], grad_up[None], grad_down[None], grad_proj, conv_input_grad)
+        conv_pre.T,
+        conv_taps,
+        out_proj,
+    )
+    return (grad_gate[None], grad_up[None], grad_down[None], grad_proj, conv_in_grad.T)
 
 
 def solution(mesh):

time: 128 us -> 110 us (0.86)
  waiting for transfers between devices: 12.2 us -> 0 us
  starting transfers between devices: 9.35 us -> 0 us
  Pallas kernels: 95 us -> 104 us
  matrix products: 2.04 us -> 0 us
  other arithmetic: 1.67 us -> 0 us
    all_to_all x1 -> x0, waiting for transfers between devices: 12.2 us -> none  [sum_at_owner(): parts = lax.all_to_all(split_up(shard, dim, peers), axis, 0, 0, tiled=True)]
    pallas_call x1, Pallas kernels: 95 us -> 104 us  [moe_call(): pl.pallas_call(functools.partial(moe_kernel, S, T), out_shape=(jax.ShapeD...]
    all_to_all x1 -> x0, starting transfers between devices: 8.06 us -> none  [sum_at_owner(): parts = lax.all_to_all(split_up(shard, dim, peers), axis, 0, 0, tiled=True)]
    dot_general x2 -> x0, matrix products: 2.04 us -> none  [the longest x1 1.75 us: body(): lax.dot_general(mid_grad, out_proj, (((1,), (1,)), ((), ())), preferred_e...]
    add x1 -> x0, other arithmetic: 1.52 us -> none  [body(): conv_input_grad + conv_taps[lag_index].astype(jnp.float32)[None, :] * ext...]
    ppermute x1 -> x0, starting transfers between devices: 1.29 us -> none  [passed_along(): lax.ppermute(value, axis, [(source, source + steps) for source in range(i...]
    unnamed x20 -> x13, local copies, waits for them, and re-layouts: 5.44 us -> 5.44 us
  transfers between devices with their start and end apart: 2 -> 0, of which waited for: 1 -> 0; matrix products, arithmetic and copies ran while one was open for 3% -> 0% of each run, Pallas kernels for 0% -> 0%
where the time goes in v2:
time: 110 us
  Pallas kernels  104 us (95%)
  local copies, waits for them, and re-layouts  5.44 us (5%)
    pallas_call x1, Pallas kernels, moe_call(): pl.pallas_call(functools.partial(moe_kernel, S, T), out_shape=(jax.ShapeD...  104 us
    unnamed x13, local copies, waits for them, and re-layouts  5.44 us

profile of v2, /device:TPU:8, one launch (start us, length us, event | category | flops | bytes accessed | tf_op | source)
XLA Modules:
  0.0 109.8 jit_solution(11235381801047962938)
XLA Ops:
  0.6 103.7 %shard_map.137 = (bf16[2048,128]{1,0:T(8,128)(2,1)}, bf16[2048,128]{1,0:T(8,128)(2,1)}, bf16[128,2048]{1,0:T(8,128)(2,1)}, f32[64,64]{1,0:T(8,128)}, f32[64,256]{1,0:T(8,128)}) custom-call(s32[2,256]{1,0:T(2,128)} %bitcast.18, f32[2,256]{1,0:T(2,128)} %bitcast.19, bf16[256,2048]{1,0:T(8,128)(2,1)} %mid.1, bf16[256,2048]{1,0:T(8,128)(2,1)} %cot.1, ...), custom_call_target="tpu_custom_call" | custom-call | tf_op jit(solution)/shard_map/pallas_call | solution.py:649
  104.4 0.0 copy-start.1
  104.4 1.9 %copy.20 = bf16[1,2048,128]{2,1,0:T(8,128)(2,1)} copy(bf16[1,2048,128]{2,1,0:T(8,128)(2,1)} %bitcast.15) | data formatting | bytes 1048576
  106.3 0.0 copy-done.1
  106.3 0.0 copy-start
  106.3 0.8 copy.21
  107.1 0.4 copy-done
  107.5 0.0 copy-start.3
  107.5 0.8 copy.22
  108.3 0.0 copy-done.3
  108.3 0.0 copy-start.2
  108.3 0.6 copy.23
  108.9 0.2 copy-done.2
  109.2 0.6 copy.24
Async XLA Ops:
  104.4 1.9 %copy-start.1 = (bf16[2048,128]{1,0:T(8,128)(2,1)S(1)}, bf16[2048,128]{1,0:T(8,128)(2,1)}, u32[]{:S(2)}) copy-start(bf16[2048,128]{1,0:T(8,128)(2,1)} %get-tuple-element.11) | copy-start | bytes 1572868
  106.3 1.2 %copy-start = (bf16[128,2048]{1,0:T(8,128)(2,1)S(1)}, bf16[128,2048]{1,0:T(8,128)(2,1)}, u32[]{:S(2)}) copy-start(bf16[128,2048]{1,0:T(8,128)(2,1)} %get-tuple-element.12) | copy-start | bytes 1572868
  107.5 0.8 copy-start.3
  108.3 0.9 copy-start.2

commit v3 on v2

v3 whole, which is shorter than its diff:
```python
import functools

import jax
import jax.numpy as jnp
from jax import lax
from jax.experimental import pallas as pl
from jax.experimental.pallas import tpu as pltpu
from jax.sharding import PartitionSpec as P

KERNEL = 31
LANES = 128
MAIN = 16
MESH = pl.DeviceIdType.MESH
F32 = jnp.float32
BF16 = jnp.bfloat16


def copy_to(src, dst, send, recv, sp, tp):
    return pltpu.make_async_remote_copy(
        src_ref=src,
        dst_ref=dst,
        send_sem=send,
        recv_sem=recv,
        device_id=(sp, tp),
        device_id_type=MESH,
    )


def moe_kernel(
    S,
    T,
    NQ,
    route_e_hbm,
    route_w_hbm,
    mid_hbm,
    cot_hbm,
    gate_hbm,
    up_hbm,
    down_hbm,
    conv_pre_hbm,
    conv_taps_hbm,
    out_proj_hbm,
    grad_gate,
    grad_up,
    grad_down,
    grad_proj,
    conv_in_grad,
    route_e,
    route_w,
    mid,
    cot,
    gate_w,
    up_w,
    down_w,
    conv_pre,
    conv_taps,
    out_proj,
    load_sem,
    send_main,
    send_ext,
    rows,
    ext,
    ext_flat,
    ext_in,
    ext_seed,
    onehot,
    onehot_x,
    hid_main,
    hid_ext,
    pre_main,
    pre_ext,
    sib_out,
    sib_in,
    own_part,
    ring_out,
    ring_in,
    back_main,
    back_ext,
    home_main,
    home_ext,
    gathered,
    mixed,
    proj_out,
    proj_in,
    halo_out,
    halo_in,
    a2a_send,
    a2a_recv,
    ag_send,
    ag_recv,
    sib_send,
    sib_recv,
    rsib_send,
    rsib_recv,
    rs_send,
    rs_recv,
    ret_send,
    ret_recv,
    mg_send,
    mg_recv,
    mgs_send,
    mgs_recv,
    proj_send,
    proj_recv,
    halo_send,
    halo_recv,
):
    Y = T // 2
    H = Y // 2
    G = Y // 4
    KQ = S // NQ
    R = S * MAIN
    RQ = KQ * MAIN
    NG = RQ + KQ
    TOK = mid.shape[1]
    CC = conv_pre.shape[0]
    HW = halo_out.shape[1]
    me = lax.axis_index("sp")
    tp = lax.axis_index("tp")
    y = tp // 2
    core = tp % 2
    sib = tp + 1 - 2 * core
    right = lax.rem(tp + 2, T)
    left = lax.rem(tp + T - 2, T)
    peers = (right, left)
    tp2 = lax.rem(tp + H * 2, T)
    mine = (tp, tp2)

    X = 4 if S >= 16 else 1
    Z = S // X
    mz = me // X
    mx = me % X

    def apart(b, sign):
        c = b // X
        zo = jnp.where(c % 2 == 1, (c + 1) // 2, -(c // 2))
        return lax.rem(mz + sign * zo + Z, Z) * X + lax.rem(mx + sign * (b % X) + X, X)

    def chunk(i, parity):
        return 2 * lax.rem(y - i + 2 * Y, Y) + parity

    def lanes(j, width=1):
        return pl.ds(pl.multiple_of(j * LANES, LANES * width), LANES * width)

    barrier = pltpu.get_barrier_semaphore()

    @pl.loop(1, S)
    def _(k):
        pl.semaphore_signal(
            barrier, inc=1, device_id=(apart(k, 1), tp), device_id_type=MESH
        )

    for peer in (left, right, sib):
        pl.semaphore_signal(barrier, inc=1, device_id=(me, peer), device_id_type=MESH)

    loads = [
        pltpu.make_async_copy(src, dst, load_sem.at[n])
        for n, (src, dst) in enumerate(
            [
                (route_e_hbm, route_e),
                (route_w_hbm, route_w),
                (mid_hbm.at[:, lanes(tp)], mid.at[0]),
                (mid_hbm.at[:, lanes(tp2)], mid.at[1]),
                (cot_hbm.at[:, lanes(tp)], cot.at[0]),
                (cot_hbm.at[:, lanes(tp2)], cot.at[1]),
                (gate_hbm, gate_w),
                (up_hbm, up_w),
                (down_hbm, down_w),
                (conv_pre_hbm, conv_pre),
                (conv_taps_hbm, conv_taps),
                (out_proj_hbm, out_proj),
            ]
        )
    ]
    for c in loads:
        c.start()
    for c in loads[0:6]:
        c.wait()

    experts = route_e[...]
    z_rel = experts // X - mz
    z_rel = jnp.where(z_rel < 0, z_rel + Z, z_rel)
    x_rel = experts % X - mx
    x_rel = jnp.where(x_rel < 0, x_rel + X, x_rel)
    turn = jnp.where(2 * z_rel <= Z, jnp.maximum(2 * z_rel - 1, 0), 2 * (Z - z_rel))
    e_rel = turn * X + x_rel
    e_iota = lax.broadcasted_iota(jnp.int32, (S, TOK), 0)
    oh = [e_iota == e_rel[k : k + 1, :] for k in range(2)]
    oh_sum = (oh[0] | oh[1]).astype(F32).astype(BF16)
    before = (
        lax.broadcasted_iota(jnp.int32, (TOK, TOK), 0)
        < lax.broadcasted_iota(jnp.int32, (TOK, TOK), 1)
    ).astype(F32).astype(BF16)
    counts = jnp.dot(oh_sum, before, preferred_element_type=F32)
    main_rows = lax.broadcasted_iota(jnp.int32, (R, TOK), 0)
    ext_rows = lax.broadcasted_iota(jnp.int32, (S, TOK), 0)
    pair_rows = lax.broadcasted_iota(jnp.int32, (2 * S, TOK), 0)
    g_main, g_ext, g_pair = [], [], []
    for k in range(2):
        rank = jnp.sum(jnp.where(oh[k], counts, 0.0), axis=0, keepdims=True).astype(jnp.int32)
        own = e_rel[k : k + 1, :]
        key = jnp.where(rank < MAIN, own * MAIN + rank, -1)
        key_x = jnp.where(rank == MAIN, own, -1)
        g_main.append(main_rows == key)
        g_ext.append(ext_rows == key_x)
        g_pair.append(pair_rows == 2 * key_x + 1)
    w = [route_w[k : k + 1, :] for k in range(2)]
    gm = (g_main[0] | g_main[1]).astype(F32).astype(BF16)
    onehot[...] = gm
    onehot_x[...] = (g_ext[0] | g_ext[1]).astype(F32).astype(BF16)
    mid_c = jnp.concatenate([mid[0], mid[1]], axis=1)
    cot_c = jnp.concatenate([cot[0], cot[1]], axis=1)
    w_main = jnp.sum(
        jnp.where(g_main[0], w[0], 0.0) + jnp.where(g_main[1], w[1], 0.0), axis=1, keepdims=True
    )
    in_rows = jnp.dot(gm, mid_c, preferred_element_type=F32).astype(BF16)
    seed_rows = (w_main * jnp.dot(gm, cot_c, preferred_element_type=F32)).astype(BF16)
    w_pair = jnp.sum(
        jnp.where(g_pair[0], w[0], 0.0) + jnp.where(g_pair[1], w[1], 0.0), axis=1, keepdims=True
    )
    g_odd = (g_pair[0] | g_pair[1]).astype(F32).astype(BF16)
    pair_even = lax.broadcasted_iota(jnp.int32, (2 * S, S), 0) == 2 * lax.broadcasted_iota(
        jnp.int32, (2 * S, S), 1
    )
    g_even = jnp.dot(
        pair_even.astype(F32).astype(BF16), onehot_x[...], preferred_element_type=F32
    ).astype(BF16)
    pair_val = (
        jnp.dot(g_even, mid_c, preferred_element_type=F32)
        + w_pair * jnp.dot(g_odd, cot_c, preferred_element_type=F32)
    ).astype(BF16)
    for m in range(2):
        part = slice(m * LANES, (m + 1) * LANES)
        send_main[m, :, 0:MAIN, :] = in_rows[:, part].reshape(S, MAIN, LANES)
        send_main[m, :, MAIN : 2 * MAIN, :] = seed_rows[:, part].reshape(S, MAIN, LANES)
        for s in range(S):
            send_ext[m, s] = pair_val[2 * s : 2 * s + 2, part]

    pl.semaphore_wait(barrier, S + 2)

    @pl.loop(1, S)
    def _(k):
        dst = apart(k, 1)
        q = k // KQ
        for m in range(2):
            for b, (src, ref) in enumerate(((send_main, rows), (send_ext, ext))):
                copy_to(
                    src.at[m, k],
                    ref.at[mine[m], k],
                    a2a_send.at[m, b],
                    a2a_recv.at[m, b, q],
                    dst,
                    tp,
                ).start()

    for m in range(2):
        rows[mine[m], 0] = send_main[m, 0]
        ext[mine[m], 0] = send_ext[m, 0]

    both = (rows, ext)
    sent = []

    def start_all(copies):
        for c in copies:
            c.start()
        sent.extend(copies)

    def sub(ref, j, q):
        return ref.at[j, pl.ds(q * KQ, KQ)]

    def ag_copies(d, t, m, q, j):
        return [
            copy_to(
                sub(ref, j, q),
                sub(ref, j, q),
                ag_send.at[d, t, m, q, b],
                ag_recv.at[d, t, m, q, b],
                me,
                peers[d],
            )
            for b, ref in enumerate(both)
        ]

    def sib_copies(i, q, j):
        return [
            copy_to(
                sub(ref, j, q), sub(ref, j, q), sib_send.at[i, q, b], sib_recv.at[i, q, b], me, sib
            )
            for b, ref in enumerate(both)
        ]

    def hops(m):
        return G - m

    def near(d, t, m):
        return ((t + 1) if d == 0 else Y - (t + 1)) + m * H

    def slot_of(i):
        return i % Y

    def step_a(q):
        lo = 1 if q == 0 else q * KQ
        n = (q + 1) * KQ - lo
        if n > 0:
            for m in range(2):
                for b, (src, ref) in enumerate(((send_main, rows), (send_ext, ext))):
                    copy_to(
                        src.at[m, pl.ds(lo, n)],
                        ref.at[mine[m], pl.ds(lo, n)],
                        a2a_send.at[m, b],
                        a2a_recv.at[m, b, q],
                        me,
                        sib,
                    ).wait_recv()
        for m in range(2):
            for d in range(2):
                if hops(m) > 0:
                    start_all(ag_copies(d, 0, m, q, mine[m]))
        for m in range(2):
            start_all(sib_copies(m * H, q, mine[m]))

    def arrive(d, t, m, q):
        i = slot_of(near(d, t, m))
        j = chunk(i, core)
        for c in ag_copies(d, t, m, q, j):
            c.wait_recv()
        if t + 1 < hops(m):
            start_all(ag_copies(d, t + 1, m, q, j))
        start_all(sib_copies(i, q, j))

    def step_f(q):
        for m in range(2):
            for d in range(2):
                if hops(m) > 0:
                    arrive(d, 0, m, q)

    def step_e(q):
        for t in range(1, G):
            for m in range(2):
                for d in range(2):
                    if t < hops(m):
                        arrive(d, t, m, q)

    sel_row = lax.broadcasted_iota(jnp.int32, (KQ, 2 * KQ), 0)
    sel_col = lax.broadcasted_iota(jnp.int32, (KQ, 2 * KQ), 1)
    sels = [(sel_col == 2 * sel_row + b).astype(F32).astype(BF16) for b in range(2)]

    def rsib_copy(q):
        return copy_to(
            sib_out.at[q, 1 - core], sib_in.at[q], rsib_send.at[q], rsib_recv.at[q], me, sib
        )

    def step_c(q):
        for i in range(Y):
            for c in sib_copies(i, q, chunk(i, 1 - core)):
                c.wait_recv()
        if q == 0:
            for c in loads[6:9]:
                c.wait()
        for j in range(T):
            for s in range(KQ):
                ext_flat[2 * s : 2 * s + 2, j * LANES : (j + 1) * LANES] = ext[j, q * KQ + s]
        flat = ext_flat[...]
        ext_q = slice(q * KQ, (q + 1) * KQ)
        x_ext = jnp.dot(sels[0], flat, preferred_element_type=F32)
        s_ext = jnp.dot(sels[1], flat, preferred_element_type=F32)
        ext_in[ext_q, :] = x_ext
        ext_seed[ext_q, :] = s_ext
        x = jnp.concatenate(
            [rows[j, q * KQ : (q + 1) * KQ, 0:MAIN, :].reshape(RQ, LANES) for j in range(T)],
            axis=1,
        )
        x = jnp.concatenate([x, x_ext.astype(BF16)], axis=0)
        g = jnp.concatenate(
            [
                rows[j, q * KQ : (q + 1) * KQ, MAIN : 2 * MAIN, :].reshape(RQ, LANES)
                for j in range(T)
            ],
            axis=1,
        )
        g = jnp.concatenate([g, s_ext.astype(BF16)], axis=0)
        w_gu = jnp.concatenate([gate_w[...], up_w[...]], axis=1)
        gate_up = jnp.dot(x, w_gu, preferred_element_type=F32)
        gate_pre = gate_up[:, 0:LANES]
        up_pre = gate_up[:, LANES : 2 * LANES]
        h_grad = lax.dot_general(
            g, down_w[...], (((1,), (1,)), ((), ())), preferred_element_type=F32
        )
        sig = jax.nn.sigmoid(gate_pre)
        act = gate_pre * sig
        hid = (act * up_pre).astype(BF16)
        gate_g = (h_grad * up_pre * (sig * (1.0 + gate_pre * (1.0 - sig)))).astype(BF16)
        pre = jnp.concatenate([gate_g, (h_grad * act).astype(BF16)], axis=1)
        hid_main[q * RQ : (q + 1) * RQ, :] = hid[0:RQ]
        hid_ext[ext_q, :] = hid[RQ:NG].astype(F32)
        pre_main[q * RQ : (q + 1) * RQ, :] = pre[0:RQ]
        pre_ext[ext_q, :] = pre[RQ:NG].astype(F32)

        parts = lax.dot_general(pre, w_gu, (((1,), (1,)), ((), ())), preferred_element_type=F32)
        for j in range(T):
            value = parts[:, j * LANES : (j + 1) * LANES]
            own_part[q, j] = value
            sib_out[q, j % 2, j // 2] = value.astype(BF16)
        start_all([rsib_copy(q)])

    def rs_copy(d, t, q):
        return copy_to(
            ring_out.at[d, t, q],
            ring_in.at[d, t, q],
            rs_send.at[d, t, q],
            rs_recv.at[d, t, q],
            me,
            peers[d],
        )

    def rs_has(d, t, q):
        if t < 0:
            return False
        return t > 0 or q % 2 == d

    def step_b(q, t):
        if t == 0:
            rsib_copy(q).wait_recv()
        if t == H:
            value = own_part[q, tp] + sib_in[q, y].astype(F32)
            for d in range(2):
                if rs_has(d, H - 1, q):
                    rs_copy(d, H - 1, q).wait_recv()
                    value = value + ring_in[d, H - 1, q].astype(F32)
            value = value.astype(BF16)
            back_main[q * KQ : (q + 1) * KQ] = value[0:RQ].reshape(KQ, MAIN, LANES)
            last = value[RQ:NG].astype(F32)
            for s in range(KQ):
                back_ext[q * KQ + s] = last[s : s + 1, :]
            if q == 0:
                home_main[0] = back_main[0]
                home_ext[0] = back_ext[0]

            @pl.loop(max(1, q * KQ), (q + 1) * KQ)
            def _(k):
                dst = apart(k, -1)
                for b, (src, ref) in enumerate(((back_main, home_main), (back_ext, home_ext))):
                    copy_to(
                        src.at[k], ref.at[k], ret_send.at[b], ret_recv.at[b], dst, tp
                    ).start()

            return
        dist = H - t
        for d in range(2):
            if not rs_has(d, t, q):
                continue
            o = dist if d == 0 else Y - dist
            to = lax.rem(y + o, Y)
            value = own_part[q, 2 * to + core] + sib_in[q, to].astype(F32)
            if rs_has(d, t - 1, q):
                rs_copy(d, t - 1, q).wait_recv()
                value = value + ring_in[d, t - 1, q].astype(F32)
            ring_out[d, t, q] = value.astype(BF16)
            start_all([rs_copy(d, t, q)])

    def weight_grads(j):
        x = jnp.concatenate(
            [rows[j, :, 0:MAIN, :].reshape(R, LANES), ext_in[:, lanes(j)].astype(BF16)], axis=0
        )
        g = jnp.concatenate(
            [
                rows[j, :, MAIN : 2 * MAIN, :].reshape(R, LANES),
                ext_seed[:, lanes(j)].astype(BF16),
            ],
            axis=0,
        )
        pre = jnp.concatenate([pre_main[...], pre_ext[...].astype(BF16)], axis=0)
        hid = jnp.concatenate([hid_main[...], hid_ext[...].astype(BF16)], axis=0)
        both_g = lax.dot_general(
            x, pre, (((0,), (0,)), ((), ())), preferred_element_type=F32
        ).astype(BF16)
        grad_gate[lanes(j), :] = both_g[:, 0:LANES]
        grad_up[lanes(j), :] = both_g[:, LANES : 2 * LANES]
        grad_down[:, lanes(j)] = lax.dot_general(
            hid, g, (((0,), (0,)), ((), ())), preferred_element_type=F32
        ).astype(BF16)

    reached = [-1] * NQ
    ready = [0]

    def round_b():
        for q in range(ready[0]):
            if reached[q] < H:
                reached[q] += 1
                step_b(q, reached[q])

    step_a(0)
    for q in range(1, NQ + 3):
        if q < NQ:
            step_a(q)
        if 0 <= q - 1 < NQ:
            step_f(q - 1)
        if 0 <= q - 2 < NQ:
            step_e(q - 2)
        if 0 <= q - 3 < NQ:
            step_c(q - 3)
            ready[0] += 1
    done = 0
    for s in range(H + 1):
        round_b()
        stop = T * (s + 1) // (H + 1)

        @pl.loop(done, stop)
        def _(j):
            weight_grads(j)

        done = stop

    for c in loads[9:12]:
        c.wait()
    pre = conv_pre[...].astype(F32)
    pre_sig = jax.nn.sigmoid(pre)
    activated = (pre * pre_sig).astype(BF16)
    eye = (
        lax.broadcasted_iota(jnp.int32, (KERNEL, KERNEL), 0)
        == lax.broadcasted_iota(jnp.int32, (KERNEL, KERNEL), 1)
    ).astype(F32).astype(BF16)
    taps = lax.dot_general(
        conv_taps[...], eye, (((0,), (0,)), ((), ())), preferred_element_type=F32
    )
    for b, (src, ref) in enumerate(((back_main, home_main), (back_ext, home_ext))):
        copy_to(
            src.at[pl.ds(1, S - 1)],
            ref.at[pl.ds(1, S - 1)],
            ret_send.at[b],
            ret_recv.at[b],
            me,
            sib,
        ).wait()
    home_x = jnp.concatenate([home_ext[s] for s in range(S)], axis=0).astype(BF16)
    moe = lax.dot_general(
        onehot[...],
        home_main[...].reshape(R, LANES),
        (((0,), (0,)), ((), ())),
        preferred_element_type=F32,
    ) + lax.dot_general(
        onehot_x[...], home_x, (((0,), (0,)), ((), ())), preferred_element_type=F32
    )
    gathered[tp] = (cot[0].astype(F32) + moe).astype(BF16)

    TH = TOK // 2

    def mg_copy(d, t, h, j):
        part = gathered.at[j, pl.ds(h * TH, TH)]
        return copy_to(part, part, mg_send.at[d, t, h], mg_recv.at[d, t, h], me, peers[d])

    def mgs_copy(i, h, j):
        part = gathered.at[j, pl.ds(h * TH, TH)]
        return copy_to(part, part, mgs_send.at[i, h], mgs_recv.at[i, h], me, sib)

    def mg_carries(d, t, h):
        if t + 1 < H:
            return True
        if t + 1 > H:
            return False
        return h == d

    mixed[...] = jnp.zeros_like(mixed)
    units = proj_out.shape[0] // S
    low = lax.broadcasted_iota(jnp.int32, (CC // 2, LANES), 1) < LANES // 2

    def use_mid(i):
        for h in range(2):
            mgs_copy(i, h, chunk(i, 1 - core)).wait_recv()
        j0 = chunk(i, 0)
        g = jnp.concatenate([gathered[j0], gathered[j0 + 1]], axis=1)
        mixed[...] += lax.dot_general(
            out_proj[:, lanes(j0, 2)], g, (((1,), (1,)), ((), ())), preferred_element_type=F32
        )
        part = jnp.dot(activated, g, preferred_element_type=F32)
        for p in range(2):
            top = part[0 : CC // 2, p * LANES : (p + 1) * LANES]
            low_c = part[CC // 2 : CC, p * LANES : (p + 1) * LANES]
            proj_out[2 * (j0 + p)] = jnp.where(
                low, top, pltpu.roll(low_c, LANES // 2, 1)
            ).astype(BF16)
            proj_out[2 * (j0 + p) + 1] = jnp.where(
                low, pltpu.roll(top, LANES // 2, 1), low_c
            ).astype(BF16)
        for p in range(4):
            u = 2 * j0 + p
            dst = u // units
            k = lax.rem(dst - me + S, S)

            @pl.when(k > 0)
            def _():
                copy_to(
                    proj_out.at[u],
                    proj_in.at[k * units + lax.rem(u, units)],
                    proj_send.at[0],
                    proj_recv.at[0],
                    dst,
                    tp,
                ).start()

    for h in range(2):
        for d in range(2):
            if mg_carries(d, 0, h):
                start_all([mg_copy(d, 0, h, tp)])
        start_all([mgs_copy(0, h, tp)])
    use_mid(0)
    for t in range(H):
        for h in range(2):
            for d in range(2):
                if not mg_carries(d, t, h):
                    continue
                i = t + 1 if d == 0 else Y - (t + 1)
                j = chunk(i, core)
                mg_copy(d, t, h, j).wait_recv()
                if mg_carries(d, t + 1, h):
                    start_all([mg_copy(d, t + 1, h, j)])
                start_all([mgs_copy(i, h, j)])
        if t + 1 < H:
            use_mid(t + 1)
            use_mid(Y - (t + 1))
        else:
            use_mid(H)

    conv_grad = (mixed[...] * (pre_sig * (1.0 + pre * (1.0 - pre_sig)))).astype(BF16)
    halo_out[...] = conv_grad[:, 0:HW]
    halo = copy_to(
        halo_out, halo_in, halo_send.at[0], halo_recv.at[0], lax.rem(me + S - 1, S), tp
    )
    start_all([halo])
    for m in range(2):
        for b, (src, ref) in enumerate(((send_main, rows), (send_ext, ext))):
            copy_to(
                src.at[m, pl.ds(1, S - 1)],
                ref.at[mine[m], pl.ds(1, S - 1)],
                a2a_send.at[m, b],
                a2a_recv.at[m, b, 0],
                me,
                sib,
            ).wait_send()
    for c in sent[:-1]:
        c.wait_send()
    halo.wait_recv()
    beyond = jnp.where(me == S - 1, 0.0, halo_in[...].astype(F32))
    extended = jnp.concatenate([conv_grad.astype(F32), beyond], axis=1)
    total = taps[:, 0:1] * extended[:, 0:TOK]
    for lag in range(1, KERNEL):
        shifted = pltpu.roll(extended, TOK + HW - lag, 1)
        total = total + taps[:, lag : lag + 1] * shifted[:, 0:TOK]
    conv_in_grad[...] = total

    copy_to(
        proj_out.at[pl.ds(units, (S - 1) * units)],
        proj_in.at[pl.ds(units, (S - 1) * units)],
        proj_send.at[0],
        proj_recv.at[0],
        me,
        sib,
    ).wait()
    for u in range(units):
        z = proj_out[me * units + u].astype(F32)
        for k in range(1, S):
            z = z + proj_in[k * units + u].astype(F32)
        tall = jnp.concatenate([z, pltpu.roll(z, LANES // 2, 1)], axis=0)
        grad_proj[u * (LANES // 2) : (u + 1) * (LANES // 2), :] = tall.T[0 : LANES // 2, :]
    halo.wait_send()


def moe_call(S, T, *args):
    Y = T // 2
    H = Y // 2
    G = max(1, Y // 4)
    TOK, D = args[2].shape
    CC = args[7].shape[0]
    NQ = min(4, S)
    KQ = S // NQ
    R = S * MAIN
    NG = KQ * MAIN + KQ
    HW = min(LANES, TOK)
    vmem = pl.BlockSpec(memory_space=pltpu.VMEM)
    hbm = pl.BlockSpec(memory_space=pltpu.HBM)
    dma = pltpu.SemaphoreType.DMA
    scratch = [
        pltpu.VMEM(args[0].shape, jnp.int32),
        pltpu.VMEM(args[1].shape, F32),
        pltpu.VMEM((2, TOK, LANES), BF16),
        pltpu.VMEM((2, TOK, LANES), BF16),
        pltpu.VMEM((D, LANES), BF16),
        pltpu.VMEM((D, LANES), BF16),
        pltpu.VMEM((LANES, D), BF16),
        pltpu.VMEM(args[7].shape, BF16),
        pltpu.VMEM(args[8].shape, BF16),
        pltpu.VMEM(args[9].shape, BF16),
        dma((12,)),
        pltpu.VMEM((2, S, 2 * MAIN, LANES), BF16),
        pltpu.VMEM((2, S, 2, LANES), BF16),
        pltpu.VMEM((T, S, 2 * MAIN, LANES), BF16),
        pltpu.VMEM((T, S, 2, LANES), BF16),
        pltpu.VMEM((2 * KQ, D), BF16),
        pltpu.VMEM((S, D), F32),
        pltpu.VMEM((S, D), F32),
        pltpu.VMEM((R, TOK), BF16),
        pltpu.VMEM((S, TOK), BF16),
        pltpu.VMEM((R, LANES), BF16),
        pltpu.VMEM((S, LANES), F32),
        pltpu.VMEM((R, 2 * LANES), BF16),
        pltpu.VMEM((S, 2 * LANES), F32),
        pltpu.VMEM((NQ, 2, Y, NG, LANES), BF16),
        pltpu.VMEM((NQ, Y, NG, LANES), BF16),
        pltpu.VMEM((NQ, T, NG, LANES), F32),
        pltpu.VMEM((2, H, NQ, NG, LANES), BF16),
        pltpu.VMEM((2, H, NQ, NG, LANES), BF16),
        pltpu.VMEM((S, MAIN, LANES), BF16),
        pltpu.VMEM((S, 1, LANES), F32),
        pltpu.VMEM((S, MAIN, LANES), BF16),
        pltpu.VMEM((S, 1, LANES), F32),
        pltpu.VMEM((T, TOK, LANES), BF16),
        pltpu.VMEM((CC, TOK), F32),
        pltpu.VMEM((2 * T, CC // 2, LANES), BF16),
        pltpu.VMEM((2 * T, CC // 2, LANES), BF16),
        pltpu.VMEM((CC, HW), BF16),
        pltpu.VMEM((CC, HW), BF16),
        dma((2, 2)),
        dma((2, 2, NQ)),
        dma((2, G, 2, NQ, 2)),
        dma((2, G, 2, NQ, 2)),
        dma((Y, NQ, 2)),
        dma((Y, NQ, 2)),
        dma((NQ,)),
        dma((NQ,)),
        dma((2, H, NQ)),
        dma((2, H, NQ)),
        dma((2,)),
        dma((2,)),
        dma((2, H, 2)),
        dma((2, H, 2)),
        dma((Y, 2)),
        dma((Y, 2)),
        dma((1,)),
        dma((1,)),
        dma((1,)),
        dma((1,)),
    ]
    return pl.pallas_call(
        functools.partial(moe_kernel, S, T, NQ),
        out_shape=(
            jax.ShapeDtypeStruct((D, LANES), BF16),
            jax.ShapeDtypeStruct((D, LANES), BF16),
            jax.ShapeDtypeStruct((LANES, D), BF16),
            jax.ShapeDtypeStruct((D // S, CC), F32),
            jax.ShapeDtypeStruct((CC, TOK), F32),
        ),
        in_specs=[hbm] * len(args),
        out_specs=(vmem,) * 5,
        scratch_shapes=scratch,
        compiler_params=pltpu.CompilerParams(
            collective_id=0, has_side_effects=True, vmem_limit_bytes=36 * 1024 * 1024
        ),
    )(*[pltpu.with_memory_space_constraint(a, pltpu.HBM) for a in args])


def body(
    S,
    T,
    mid_state,
    conv_pre,
    conv_taps,
    out_proj,
    route_expert,
    route_weight,
    gate_w,
    up_w,
    down_w,
    cotangent,
):
    grad_gate, grad_up, grad_down, grad_proj, conv_in_grad = moe_call(
        S,
        T,
        route_expert.T,
        route_weight.T,
        mid_state,
        cotangent,
        gate_w[0],
        up_w[0],
        down_w[0],
        conv_pre.T,
        conv_taps,
        out_proj,
    )
    return (grad_gate[None], grad_up[None], grad_down[None], grad_proj, conv_in_grad.T)


def solution(mesh):
    placed = (
        P("sp", None),
        P("sp", "tp"),
        P(None, "tp"),
        P("tp", None),
        P("sp", None),
        P("sp", None),
        P("sp", None, "tp"),
        P("sp", None, "tp"),
        P("sp", "tp", None),
        P("sp", None),
    )
    return jax.shard_map(
        functools.partial(body, mesh.shape["sp"], mesh.shape["tp"]),
        mesh=mesh,
        in_specs=placed,
        out_specs=(
            P("sp", None, "tp"),
            P("sp", None, "tp"),
            P("sp", "tp", None),
            P("sp", "tp"),
            P("sp", "tp"),
        ),
        check_vma=False,
    )
```

time: 110 us -> 94.5 us (0.86)
  the two profiles are of different devices: /device:TPU:8 before, /device:TPU:31 now
where the time goes in v3:
time: 94.5 us; the launch traced here: 94.4 us
  Pallas kernels  90.1 us (95%)
  local copies, waits for them, and re-layouts  3.62 us (4%)
    pallas_call x1, Pallas kernels, moe_call(): pl.pallas_call(functools.partial(moe_kernel, S, T, NQ), out_shape=(jax.Sh...  90.1 us
    unnamed x5, local copies, waits for them, and re-layouts  3.62 us

profile of v3, /device:TPU:31, one launch (start us, length us, event | category | flops | bytes accessed | tf_op | source)
XLA Modules:
  0.0 94.4 jit_solution(17992540393268453796)
XLA Ops:
  0.6 90.1 %shard_map.137 = (bf16[2048,128]{1,0:T(8,128)(2,1)S(1)}, bf16[2048,128]{1,0:T(8,128)(2,1)S(1)}, bf16[128,2048]{1,0:T(8,128)(2,1)S(1)}, f32[64,64]{1,0:T(8,128)S(1)}, f32[64,256]{1,0:T(8,128)S(1)}) custom-call(s32[2,256]{1,0:T(2,128)} %bitcast.18, f32[2,256]{1,0:T(2,128)} %bitcast.19, bf16[256,2048]{1,0:T(8,128)(2,1)} %mid_hbm.1, bf16[256,2048]{1,0:T(8,128)(2,1)} %cot_hbm.1, ...), custom_call_target="tpu_custom_call" | custom-call | tf_op jit(solution)/shard_map/pallas_call | solution.py:743
  90.8 0.8 copy.20
  91.6 0.8 copy.21
  92.4 0.8 copy.22
  93.2 0.6 copy.23
  93.8 0.6 copy.24

commit v4 on v3

--- a/solution.py
+++ b/solution.py
@@ -123,6 +123,7 @@
     right = lax.rem(tp + 2, T)
     left = lax.rem(tp + T - 2, T)
     peers = (right, left)
+    peers2 = (lax.rem(tp + 4, T), lax.rem(tp + T - 4 + T, T))
     tp2 = lax.rem(tp + H * 2, T)
     mine = (tp, tp2)
 
@@ -150,7 +151,7 @@
             barrier, inc=1, device_id=(apart(k, 1), tp), device_id_type=MESH
         )
 
-    for peer in (left, right, sib):
+    for peer in (left, right, sib) + (peers2 if H > 1 else ()):
         pl.semaphore_signal(barrier, inc=1, device_id=(me, peer), device_id_type=MESH)
 
     loads = [
@@ -236,7 +237,7 @@
         for s in range(S):
             send_ext[m, s] = pair_val[2 * s : 2 * s + 2, part]
 
-    pl.semaphore_wait(barrier, S + 2)
+    pl.semaphore_wait(barrier, S + 2 + (2 if H > 1 else 0))
 
     @pl.loop(1, S)
     def _(k):
@@ -545,9 +546,10 @@
 
     TH = TOK // 2
 
-    def mg_copy(d, t, h, j):
+    def mg_copy(d, t, h, j, hop):
         part = gathered.at[j, pl.ds(h * TH, TH)]
-        return copy_to(part, part, mg_send.at[d, t, h], mg_recv.at[d, t, h], me, peers[d])
+        peer = peers[d] if hop == 1 else peers2[d]
+        return copy_to(part, part, mg_send.at[d, t, h], mg_recv.at[d, t, h], me, peer)
 
     def mgs_copy(i, h, j):
         part = gathered.at[j, pl.ds(h * TH, TH)]
@@ -598,11 +600,13 @@
                     tp,
                 ).start()
 
-    for h in range(2):
-        for d in range(2):
-            if mg_carries(d, 0, h):
-                start_all([mg_copy(d, 0, h, tp)])
-        start_all([mgs_copy(0, h, tp)])
+    for hop in range(1, 3):
+        for h in range(2):
+            for d in range(2):
+                if mg_carries(d, hop - 1, h):
+                    start_all([mg_copy(d, hop - 1, h, tp, hop)])
+            if hop == 1:
+                start_all([mgs_copy(0, h, tp)])
     use_mid(0)
     for t in range(H):
         for h in range(2):
@@ -611,15 +615,16 @@
                     continue
                 i = t + 1 if d == 0 else Y - (t + 1)
                 j = chunk(i, core)
-                mg_copy(d, t, h, j).wait_recv()
-                if mg_carries(d, t + 1, h):
-                    start_all([mg_copy(d, t + 1, h, j)])
+                mg_copy(d, t, h, j, 1).wait_recv()
+                if t == 1:
+                    for hop in range(1, 3):
+                        if mg_carries(d, t + hop, h):
+                            start_all([mg_copy(d, t + hop, h, j, hop)])
                 start_all([mgs_copy(i, h, j)])
-        if t + 1 < H:
-            use_mid(t + 1)
-            use_mid(Y - (t + 1))
-        else:
-            use_mid(H)
+        if t > 0:
+            use_mid(t)
+            use_mid(Y - t)
+    use_mid(H)
 
     conv_grad = (mixed[...] * (pre_sig * (1.0 + pre * (1.0 - pre_sig)))).astype(BF16)
     halo_out[...] = conv_grad[:, 0:HW]
@@ -758,6 +763,28 @@
     )(*[pltpu.with_memory_space_constraint(a, pltpu.HBM) for a in args])
 
 
+def settle_kernel(*refs):
+    n = len(refs) // 2
+    copies = [
+        pltpu.make_async_copy(refs[k], refs[n + k], refs[-1].at[k]) for k in range(n)
+    ]
+    for c in copies:
+        c.start()
+    for c in copies:
+        c.wait()
+
+
+def settle(*arrays):
+    return pl.pallas_call(
+        settle_kernel,
+        out_shape=tuple(jax.ShapeDtypeStruct(a.shape, a.dtype) for a in arrays),
+        in_specs=[pl.BlockSpec(memory_space=pltpu.VMEM)] * len(arrays),
+        out_specs=(pl.BlockSpec(memory_space=pltpu.HBM),) * len(arrays),
+        scratch_shapes=[pltpu.SemaphoreType.DMA((len(arrays),))],
+        compiler_params=pltpu.CompilerParams(vmem_limit_bytes=8 * 1024 * 1024),
+    )(*arrays)
+
+
 def body(
     S,
     T,
@@ -772,7 +799,7 @@
     down_w,
     cotangent,
 ):
-    grad_gate, grad_up, grad_down, grad_proj, conv_in_grad = moe_call(
+    results = moe_call(
         S,
         T,
         route_expert.T,
@@ -786,6 +813,7 @@
         conv_taps,
         out_proj,
     )
+    grad_gate, grad_up, grad_down, grad_proj, conv_in_grad = settle(*results)
     return (grad_gate[None], grad_up[None], grad_down[None], grad_proj, conv_in_grad.T)
 
 

time: 94.5 us -> 90.9 us (0.962)
  the two profiles are of different devices: /device:TPU:31 before, /device:TPU:22 now
where the time goes in v4:
time: 90.9 us; the launch traced here: 90.7 us
  Pallas kernels  90.1 us (99%)
    pallas_call x1, Pallas kernels, moe_call(): pl.pallas_call(functools.partial(moe_kernel, S, T, NQ), out_shape=(jax.Sh...  88.9 us

profile of v4, /device:TPU:22, one launch (start us, length us, event | category | flops | bytes accessed | tf_op | source)
XLA Modules:
  0.0 90.7 jit_solution(731355164867458167)
XLA Ops:
  0.6 88.9 %shard_map.137 = (bf16[2048,128]{1,0:T(8,128)(2,1)S(1)}, bf16[2048,128]{1,0:T(8,128)(2,1)S(1)}, bf16[128,2048]{1,0:T(8,128)(2,1)S(1)}, f32[64,64]{1,0:T(8,128)S(1)}, f32[64,256]{1,0:T(8,128)S(1)}) custom-call(s32[2,256]{1,0:T(2,128)} %bitcast.14, f32[2,256]{1,0:T(2,128)} %bitcast.15, bf16[256,2048]{1,0:T(8,128)(2,1)} %mid_hbm.1, bf16[256,2048]{1,0:T(8,128)(2,1)} %cot_hbm.1, ...), custom_call_target="tpu_custom_call" | custom-call | tf_op jit(solution)/shard_map/pallas_call | solution.py:748
  89.5 1.2 %shard_map.138 = (bf16[2048,128]{1,0:T(8,128)(2,1)}, bf16[2048,128]{1,0:T(8,128)(2,1)}, bf16[128,2048]{1,0:T(8,128)(2,1)}, f32[64,64]{1,0:T(8,128)}, f32[64,256]{1,0:T(8,128)}) custom-call(bf16[2048,128]{1,0:T(8,128)(2,1)S(1)} %get-tuple-element.15.refs_0_, bf16[2048,128]{1,0:T(8,128)(2,1)S(1)} %get-tuple-element.16.refs_1_, ...), custom_call_target="tpu_custom_call" | custom-call | tf_op jit(solution)/shard_map/pallas_call | solution.py:778

commit v5 on v4

--- a/solution.py
+++ b/solution.py
@@ -600,7 +600,7 @@
                     tp,
                 ).start()
 
-    for hop in range(1, 3):
+    for hop in (2, 1):
         for h in range(2):
             for d in range(2):
                 if mg_carries(d, hop - 1, h):
@@ -617,7 +617,7 @@
                 j = chunk(i, core)
                 mg_copy(d, t, h, j, 1).wait_recv()
                 if t == 1:
-                    for hop in range(1, 3):
+                    for hop in (2, 1):
                         if mg_carries(d, t + hop, h):
                             start_all([mg_copy(d, t + hop, h, j, hop)])
                 start_all([mgs_copy(i, h, j)])

time: 90.9 us -> 91.7 us (level)
  the two profiles are of different devices: /device:TPU:22 before, /device:TPU:30 now
where the time goes in v5:
time: 91.7 us; the launch traced here: 91.6 us
  Pallas kernels  90.9 us (99%)
    pallas_call x1, Pallas kernels, moe_call(): pl.pallas_call(functools.partial(moe_kernel, S, T, NQ), out_shape=(jax.Sh...  89.7 us

profile of v5, /device:TPU:30, one launch (start us, length us, event | category | flops | bytes accessed | tf_op | source)
XLA Modules:
  0.0 91.6 jit_solution(9179904567289746303)
XLA Ops:
  0.6 89.7 %shard_map.137 = (bf16[2048,128]{1,0:T(8,128)(2,1)S(1)}, bf16[2048,128]{1,0:T(8,128)(2,1)S(1)}, bf16[128,2048]{1,0:T(8,128)(2,1)S(1)}, f32[64,64]{1,0:T(8,128)S(1)}, f32[64,256]{1,0:T(8,128)S(1)}) custom-call(s32[2,256]{1,0:T(2,128)} %bitcast.14, f32[2,256]{1,0:T(2,128)} %bitcast.15, bf16[256,2048]{1,0:T(8,128)(2,1)} %mid_hbm.1, bf16[256,2048]{1,0:T(8,128)(2,1)} %cot_hbm.1, ...), custom_call_target="tpu_custom_call" | custom-call | tf_op jit(solution)/shard_map/pallas_call | solution.py:748
  90.3 1.2 %shard_map.138 = (bf16[2048,128]{1,0:T(8,128)(2,1)}, bf16[2048,128]{1,0:T(8,128)(2,1)}, bf16[128,2048]{1,0:T(8,128)(2,1)}, f32[64,64]{1,0:T(8,128)}, f32[64,256]{1,0:T(8,128)}) custom-call(bf16[2048,128]{1,0:T(8,128)(2,1)S(1)} %get-tuple-element.15.refs_0_, bf16[2048,128]{1,0:T(8,128)(2,1)S(1)} %get-tuple-element.16.refs_1_, ...), custom_call_target="tpu_custom_call" | custom-call | tf_op jit(solution)/shard_map/pallas_call | solution.py:778
